TPU v7x, 32 devices: a whole 2x2x4 slice. The times are simulated.
32 devices in a mesh: ep: 8 (over z, y), tp: 4 (over x, core).
Axes of the slice: x: 2, y: 2, z: 4, core: 2. Of those that a mesh axis runs over, the one named last changes fastest.
Arguments:
- query_latent: bfloat16 [1024, 768], P('ep'), may hold values from -6 to 6
- keyval_latent: bfloat16 [1024, 512], P('ep'), may hold values from -6 to 6
- rotary_key: bfloat16 [1024, 32], P('ep'), may hold values from -6 to 6
- query_gain: float32 [768], replicated, may hold values from 0.3 to 48
- keyval_gain: float32 [512], replicated, may hold values from 0.1 to 1.9
- query_weight: bfloat16 [768, 1536], P(None, 'tp'), may hold values from -0.21875 to 0.21875
- keyval_weight: bfloat16 [512, 2048], P(None, 'tp'), may hold values from -0.25 to 0.25
- output_weight: bfloat16 [1024, 2048], P('tp'), may hold values from -0.1875 to 0.1875
- output_gain: float32 [2048], replicated, may hold values from 0.1 to 1.9
- second_rows: bfloat16 [1024, 2048], P('ep'), may hold values from -6 to 6
- second_gain: float32 [2048], replicated, may hold values from 0.1 to 1.9
- route_ids: int32 [1024, 4], P('ep'), may hold values from 0 to 7, all different within a row; in each aligned block of 128 rows (0 to 127, 128 to 255, ...) at most 128 rows name the same one
- route_weights: float32 [1024, 4], P('ep'), may hold values from 0.1 to 1
- gate_weight: bfloat16 [8, 2048, 1024], P('ep', None, 'tp'), may hold values from -0.125 to 0.125
- up_weight: bfloat16 [8, 2048, 1024], P('ep', None, 'tp'), may hold values from -0.125 to 0.125
- down_weight: bfloat16 [8, 1024, 2048], P('ep', 'tp'), may hold values from -0.1875 to 0.1875
- shared_gate: bfloat16 [2048, 512], P(None, 'tp'), may hold values from -0.125 to 0.125
- shared_up: bfloat16 [2048, 512], P(None, 'tp'), may hold values from -0.125 to 0.125
- shared_down: bfloat16 [512, 2048], P('tp'), may hold values from -0.25 to 0.25
Outputs:
- mixed: bfloat16 [1024, 2048], P(('ep', 'tp'))
- expert_mix: bfloat16 [1024, 2048], P('ep', 'tp')
Inputs may be any that keep to these rules, and one draw needn't show every extreme that they name: `route_ids`: each row names 4 different experts. Among the rows of one index of ep (aligned blocks of 128 rows) no expert is named more than 128 times, a bound that some expert reaches in some blocks.
All inputs are finite; a program needn't handle non-finite values.
Results may differ from a plain program's by a relative error of at most 0.023.
The roundings to bfloat16 on the way count: a program that leaves them out, or rounds other values in their place, can miss the bound.
Values may be sent and summed in bfloat16 or wider, within the bound.
No kernel may reach another device: no remote copies, remote signals or barrier semaphores. Data moves between devices by JAX's collectives and lax.ppermute only.
A program may use at most 128 MiB of HBM per device.

v0:
```python
import functools

import jax
import jax.numpy as jnp
import numpy as np
from jax import lax
from jax.experimental import pallas as pl
from jax.experimental.pallas import tpu as pltpu
from jax.sharding import PartitionSpec as P

NOPE = 64
ROPE = 32
VDIM = 64
LANES = 128


EPS = 1e-06
ROPE_BASE = 10000.0


VMEM = pl.BlockSpec(memory_space=pltpu.VMEM)
MIB = 2**20


def within(mib):
    return pltpu.CompilerParams(vmem_limit_bytes=mib * MIB)


def rms_scale(values, gain_vec):
    widened = values.astype(jnp.float32)
    normed = widened * lax.rsqrt(jnp.mean(widened * widened, -1, keepdims=True) + EPS)
    return (normed * gain_vec).astype(jnp.bfloat16)


def swap(values, axis, mask):
    count = lax.axis_size(axis)
    return lax.ppermute(values, axis, [(i, i ^ mask) for i in range(count)])


def dot32(left, right):
    return jnp.dot(left, right, preferred_element_type=jnp.float32)


def dot32_t(left, right):
    return lax.dot_general(left, right, (((1,), (1,)), ((), ())), preferred_element_type=jnp.float32)


def gated(rows, gate, up):
    gate_act = dot32(rows, gate)
    return gate_act / (1.0 + jnp.exp(-gate_act)) * dot32(rows, up)


def token_kernel(rows, gain, ids, weights, out, table, *, expert_count):
    half = out.shape[0]
    width = rows.shape[1]
    start = pl.multiple_of(lax.axis_index("tp") % 2 * half, half)
    out[:, :width] = rms_scale(rows[pl.ds(start, half), :], gain[...])
    spots = lax.broadcasted_iota(jnp.int32, (out.shape[1] - width, rows.shape[0]), 0)
    low = spots >= expert_count
    expert = jnp.where(low, spots - expert_count, spots)
    factor = jnp.zeros(spots.shape, jnp.float32)
    for k in range(ids.shape[0]):
        factor = factor + jnp.where(ids[k : k + 1, :] == expert, weights[k : k + 1, :], 0.0)
    high = factor.astype(jnp.bfloat16).astype(jnp.float32)
    table[...] = jnp.where(low, factor - high, high).T
    out[:, width:] = table[pl.ds(start, half), :].astype(jnp.bfloat16)


def key_kernel(latent, gain, rotary, cosine, sine, spread, out, both):
    half = out.shape[0]
    width = latent.shape[1]
    start = pl.multiple_of(lax.axis_index("tp") % 2 * half, half)
    out[:, :width] = rms_scale(latent[pl.ds(start, half), :], gain[...])
    both[...] = lax.dot_general(
        rotary[...], spread[...], (((0,), (0,)), ((), ())), preferred_element_type=jnp.float32
    )
    turned = both.shape[1] // 2
    out[:, width:] = (
        both[pl.ds(start, half), :turned] * cosine[pl.ds(start, half), :]
        + both[pl.ds(start, half), turned:] * sine[pl.ds(start, half), :]
    ).astype(jnp.bfloat16)


def query_kernel(latent, gain, weight, order, cosine, sine, out):
    turned = cosine.shape[1]
    plain = out.shape[1] - turned
    ordered = dot32(weight[...], order[...]).astype(jnp.bfloat16)
    both = dot32(rms_scale(latent[...], gain[...]), ordered)
    out[:, :plain] = both[:, :plain].astype(jnp.bfloat16)
    out[:, plain:] = (
        both[:, plain : plain + turned] * cosine[...] + both[:, plain + turned :] * sine[...]
    ).astype(jnp.bfloat16)


def attention_kernel(queries, *refs, head_count, piece_count, tp_count):
    pieces = refs[:piece_count]
    key_weight, out_weight, keep, send, part = refs[piece_count:]
    latent_width = key_weight.shape[0]
    plain = head_count * (NOPE + VDIM)
    scale = (NOPE + ROPE) ** (-0.5)
    rows = queries.shape[0]
    keyvals = [dot32(p[:, :latent_width], key_weight[...]).astype(jnp.bfloat16) for p in pieces]
    turned_queries = queries[:, plain:]
    spots = lax.broadcasted_iota(jnp.int32, turned_queries.shape, 1)
    lane = lax.broadcasted_iota(jnp.int32, (rows, NOPE + VDIM), 1)
    heads = []
    for h in range(head_count):
        cols = slice(h * (NOPE + VDIM), (h + 1) * (NOPE + VDIM))
        own = (spots >= h * ROPE) & (spots < (h + 1) * ROPE)
        turned = jnp.where(own, turned_queries.astype(jnp.float32), 0.0).astype(jnp.bfloat16)
        scores = [
            (
                dot32_t(queries[:, cols], keyvals[i][:, cols])
                + dot32_t(turned, pieces[i][:, latent_width:])
            )
            * scale
            for i in range(piece_count)
        ]
        top = functools.reduce(
            jnp.maximum, [jnp.max(s, -1, keepdims=True) for s in scores]
        )
        total = jnp.zeros((rows, 1), jnp.float32)
        summed = jnp.zeros((rows, NOPE + VDIM), jnp.float32)
        for i in range(piece_count):
            exponent = jnp.exp(scores[i] - top)
            total = total + jnp.sum(exponent, -1, keepdims=True)
            summed = summed + dot32(exponent.astype(jnp.bfloat16), keyvals[i][:, cols])
        heads.append(summed / total)
    pairs = [
        jnp.where(lane < NOPE, pltpu.roll(heads[h], NOPE, 1), heads[h + 1]).astype(jnp.bfloat16)
        for h in range(0, head_count, 2)
    ]
    part[...] = dot32(jnp.concatenate(pairs, 1), out_weight[...])
    quarter = rows // tp_count
    core = lax.axis_index("tp") % 2
    side = lax.axis_index("tp") // 2
    for at in range(tp_count // 2):
        row = side if at == 0 else 1 - side
        here = pl.multiple_of((row * 2 + core) * quarter, quarter)
        there = pl.multiple_of((row * 2 + 1 - core) * quarter, quarter)
        span = slice(at * quarter, (at + 1) * quarter)
        keep[span, :] = part[pl.ds(here, quarter), :]
        send[span, :] = part[pl.ds(there, quarter), :].astype(jnp.bfloat16)


def expert_kernel(upper, lower, *refs, held_count, stream_count, expert_count):
    held = refs[:held_count]
    hbm = refs[held_count : held_count + stream_count]
    keep, send, part = refs[held_count + stream_count : held_count + stream_count + 3]
    copies = []
    if stream_count:
        sems = refs[-stream_count - 1]
        landed = refs[-stream_count:]
        copies = [
            pltpu.make_async_copy(hbm[i], landed[i], sems.at[i]) for i in range(stream_count)
        ]
        for copy in copies:
            copy.start()
    half = upper.shape[0]
    width = part.shape[1]
    rows = jnp.concatenate([upper[:, :width], lower[:, :width]], 0)
    scale = jnp.concatenate([upper[:, width:], lower[:, width:]], 0).astype(jnp.float32)
    spots = lax.broadcasted_iota(jnp.int32, scale.shape, 1)
    local_count = held[0].shape[0]

    def routed(gate, up, down):
        total = None
        for i in range(local_count):
            mine = lax.axis_index("ep") * local_count + i
            hot = (spots == mine) | (spots == mine + expert_count)
            factor = jnp.sum(jnp.where(hot, scale, 0.0), 1, keepdims=True)
            hidden = (gated(rows, gate[i], up[i]) * factor).astype(jnp.bfloat16)
            term = dot32(hidden, down[i])
            total = term if total is None else total + term
        return total

    total = routed(*held[:3])
    for at in range(3, held_count, 3):
        total = total + routed(*held[at : at + 3])
    part[...] = total
    for at in range(0, stream_count, 3):
        for copy in copies[at : at + 3]:
            copy.wait()
        gate, up, down = landed[at : at + 3]
        if at < stream_count - 3:
            hidden = gated(rows[:half], gate[...], up[...]).astype(jnp.bfloat16)
            part[:half, :] = part[:half, :] + dot32(hidden, down[...])
        else:
            part[...] = part[...] + routed(gate, up, down)
    column = keep.shape[1]
    side = lax.axis_index("tp") // 2
    here = pl.multiple_of(side * column, column)
    there = pl.multiple_of((1 - side) * column, column)
    keep[...] = part[:, pl.ds(here, column)]
    send[...] = part[:, pl.ds(there, column)].astype(jnp.bfloat16)


def call_experts(upper, lower, held, streamed, model_width, expert_count):
    rows = upper.shape[0] + lower.shape[0]
    column = model_width // 2
    scratch = [pltpu.VMEM((rows, model_width), jnp.float32)]
    if streamed:
        scratch += [pltpu.SemaphoreType.DMA((len(streamed),))]
        scratch += [pltpu.VMEM(w.shape, w.dtype) for w in streamed]
    return pl.pallas_call(
        functools.partial(
            expert_kernel,
            held_count=len(held),
            stream_count=len(streamed),
            expert_count=expert_count,
        ),
        out_shape=(
            jax.ShapeDtypeStruct((rows, column), jnp.float32),
            jax.ShapeDtypeStruct((rows, column), jnp.bfloat16),
        ),
        in_specs=[VMEM] * (2 + len(held)) + [pl.BlockSpec(memory_space=pltpu.HBM)] * len(streamed),
        out_specs=(VMEM, VMEM),
        scratch_shapes=scratch,
        compiler_params=within(16),
        name="experts",
    )(upper, lower, *held, *[pltpu.with_memory_space_constraint(w, pltpu.HBM) for w in streamed])


def column_order(head_count):
    step = NOPE + ROPE
    half = ROPE // 2
    turned = head_count * ROPE
    plain = head_count * (NOPE + VDIM)
    order = np.zeros((head_count * step, plain + 2 * turned), np.float32)
    for h in range(head_count):
        for i in range(NOPE):
            order[h * step + i, h * (NOPE + VDIM) + i] = 1.0
        for i in range(ROPE):
            at = plain + h * ROPE + i
            order[h * step + NOPE + i, at] = 1.0
            if i < half:
                order[h * step + NOPE + half + i, at + turned] = -1.0
            else:
                order[h * step + NOPE + i - half, at + turned] = 1.0
    return order


def key_spread(head_count):
    half = ROPE // 2
    turned = head_count * ROPE
    spread = np.zeros((ROPE, 2 * turned), np.float32)
    for h in range(head_count):
        for i in range(ROPE):
            at = h * ROPE + i
            spread[i, at] = 1.0
            if i < half:
                spread[half + i, at + turned] = -1.0
            else:
                spread[i - half, at + turned] = 1.0
    return spread


def far_order(far_count):
    return [0] + [k for k in (2, 1) if k < far_count] + list(range(3, far_count))


def per_device(
    query_latent,
    keyval_latent,
    rotary_key,
    query_gain,
    keyval_gain,
    query_weight,
    keyval_weight,
    output_weight,
    output_gain,
    second_rows,
    second_gain,
    route_ids,
    route_weights,
    gate_weight,
    up_weight,
    down_weight,
    shared_gate,
    shared_up,
    shared_down,
):
    tp_count = lax.axis_size("tp")
    ep_count = lax.axis_size("ep")
    far_count = ep_count // 2
    own_tp = lax.axis_index("tp")
    own_ep = lax.axis_index("ep")
    core = own_tp % 2
    local_count = gate_weight.shape[0]
    expert_count = local_count * ep_count

    tok_rows, model_width = second_rows.shape
    half_rows = tok_rows // 2
    tail_width = -(-2 * expert_count // LANES) * LANES
    unit = pl.pallas_call(
        functools.partial(token_kernel, expert_count=expert_count),
        out_shape=jax.ShapeDtypeStruct((half_rows, model_width + tail_width), jnp.bfloat16),
        in_specs=[VMEM] * 4,
        out_specs=VMEM,
        scratch_shapes=[pltpu.VMEM((tok_rows, tail_width), jnp.float32)],
        name="tokens",
    )(second_rows, second_gain.reshape(1, -1), route_ids.T, route_weights.T)

    far_units = [unit]
    for k in range(1, far_count):
        far_units.append(swap(unit, "ep", 2 * k))
    near_units = [swap(u, "ep", 1) for u in far_units]

    first_rows = query_latent.shape[0]
    half_keys = first_rows // 2
    head_count = query_weight.shape[1] // (NOPE + ROPE)
    turned = head_count * ROPE
    lane_pair = np.arange(turned) % (ROPE // 2)
    inverse = 1.0 / ROPE_BASE ** (lane_pair.astype(np.float32) * 2.0 / ROPE)
    positions = (own_ep * first_rows).astype(jnp.float32) + jnp.arange(
        first_rows, dtype=jnp.float32
    )
    angles = positions[:, None] * jnp.asarray(inverse, jnp.float32)[None, :]
    cosine = jnp.cos(angles)
    sine = jnp.sin(angles)
    latent_width = keyval_latent.shape[1]
    key_unit = pl.pallas_call(
        key_kernel,
        out_shape=jax.ShapeDtypeStruct((half_keys, latent_width + turned), jnp.bfloat16),
        in_specs=[VMEM] * 6,
        out_specs=VMEM,
        scratch_shapes=[pltpu.VMEM((first_rows, 2 * turned), jnp.float32)],
        name="keys",
    )(
        keyval_latent,
        keyval_gain.reshape(1, -1),
        rotary_key.T,
        cosine,
        sine,
        jnp.asarray(key_spread(head_count), jnp.bfloat16),
    )
    far_keys = jnp.concatenate(
        [key_unit] + [swap(key_unit, "ep", 2 * k) for k in range(1, far_count)], 0
    )
    near_keys = swap(far_keys, "ep", 1)
    pieces = [far_keys, near_keys, swap(far_keys, "tp", 1), swap(near_keys, "tp", 1)]

    own_shared = (shared_gate, shared_up, shared_down)
    own_routed = (gate_weight, up_weight, down_weight)
    other_shared = tuple(swap(w, "tp", 1) for w in own_shared)
    other_routed = tuple(swap(w, "tp", 1) for w in own_routed)

    queries = pl.pallas_call(
        query_kernel,
        out_shape=jax.ShapeDtypeStruct(
            (first_rows, head_count * (NOPE + VDIM) + turned), jnp.bfloat16
        ),
        in_specs=[VMEM] * 6,
        out_specs=VMEM,
        compiler_params=within(12),
        name="queries",
    )(
        query_latent,
        query_gain.reshape(1, -1),
        query_weight,
        jnp.asarray(column_order(head_count), jnp.bfloat16),
        cosine,
        sine,
    )

    arrived = None
    for k in far_order(far_count):
        keep, send = call_experts(
            far_units[k],
            near_units[k],
            other_routed + own_routed if k else other_routed,
            () if k else own_shared + other_shared + own_routed,
            model_width,
            expert_count,
        )
        got = swap(send, "tp", 2)
        lower = (keep[half_rows:] + got[half_rows:].astype(jnp.float32)).astype(jnp.bfloat16)
        upper = keep[:half_rows] + got[:half_rows].astype(jnp.float32)
        total = upper + swap(lower, "ep", 1).astype(jnp.float32)
        if k:
            total = swap(total.astype(jnp.bfloat16), "ep", 2 * k).astype(jnp.float32)
        arrived = total if arrived is None else arrived + total
    quarter_width = model_width // 4
    mine = lax.dynamic_slice_in_dim(arrived, core * quarter_width, quarter_width, 1)
    other = lax.dynamic_slice_in_dim(arrived, (1 - core) * quarter_width, quarter_width, 1)
    mine = mine.astype(jnp.bfloat16)
    other = swap(other.astype(jnp.bfloat16), "tp", 1)
    first = core == 0
    expert_mix = jnp.concatenate(
        [jnp.where(first, mine, other), jnp.where(first, other, mine)], 0
    )

    quarter = first_rows // tp_count
    keep, send = pl.pallas_call(
        functools.partial(
            attention_kernel, head_count=head_count, piece_count=len(pieces), tp_count=tp_count
        ),
        out_shape=(
            jax.ShapeDtypeStruct((first_rows // 2, model_width), jnp.float32),
            jax.ShapeDtypeStruct((first_rows // 2, model_width), jnp.bfloat16),
        ),
        in_specs=[VMEM] * (len(pieces) + 3),
        out_specs=(VMEM, VMEM),
        scratch_shapes=[pltpu.VMEM((first_rows, model_width), jnp.float32)],
        compiler_params=within(10 + ep_count * first_rows // 200),
        name="attention",
    )(queries, *pieces, keyval_weight, output_weight)
    got = swap(send, "tp", 1)
    given = (keep[quarter:] + got[quarter:].astype(jnp.float32)).astype(jnp.bfloat16)
    mixture = keep[:quarter] + got[:quarter].astype(jnp.float32)
    mixture = mixture + swap(given, "tp", 2).astype(jnp.float32)
    mixed = rms_scale(mixture, output_gain)
    return (mixed, expert_mix)


def solution(mesh):
    placed = (
        P("ep", None),
        P("ep", None),
        P("ep", None),
        P(),
        P(),
        P(None, "tp"),
        P(None, "tp"),
        P("tp", None),
        P(),
        P("ep", None),
        P(),
        P("ep", None),
        P("ep", None),
        P("ep", None, "tp"),
        P("ep", None, "tp"),
        P("ep", "tp", None),
        P(None, "tp"),
        P(None, "tp"),
        P("tp", None),
    )

    return jax.shard_map(
        per_device,
        mesh=mesh,
        in_specs=placed,
        out_specs=(P(("ep", "tp"), None), P("ep", "tp")),
        check_vma=False,
    )
```

profile of v0, /device:TPU:0, one launch (start us, length us, event | category | flops | bytes accessed | tf_op | source)
XLA Modules:
  0.0 131.0 jit_solution(15868414770205237190)
XLA Ops:
  2.2 1.8 %keys.1 = bf16[64,640]{1,0:T(8,128)(2,1)} custom-call(bf16[128,512]{1,0:T(8,128)(2,1)} %latent.3, f32[1,512]{1,0:T(1,128)} %bitcast.7, bf16[32,128]{1,0:T(8,128)(2,1)} %bitcast.6, f32[128,128]{1,0:T(8,128)} %get-tuple-element.25.cosine, f32[128,128]{1,0:T(8,128)} %get-tuple-element.24.sine, bf16[32,256]{1,0:T(8,128)(2,1)} %constant.44.clone.spread), custom_call_target="tpu_custom_call" | custom-call | tf_op jit(solution)/shard_map/keys/pallas_call | solution.py:322
  4.1 3.1 %collective-permute-start = (bf16[64,640]{1,0:T(8,128)(2,1)}, bf16[64,640]{1,0:T(8,128)(2,1)S(1)}, u32[]{:S(2)}, u32[]{:S(2)}) collective-permute-start(bf16[64,640]{1,0:T(8,128)(2,1)} %keys.1), channel_id=1, source_target_pairs={{0,8},{4,12},{8,0},{12,4},{16,24},{20,28},{24,16},{28,20},{1,9},{5... | collective-permute-start | bytes 245768 | tf_op jit(solution)/shard_map/ppermute | solution.py:37
  7.1 2.0 %tokens.1.upper = bf16[64,2176]{1,0:T(8,128)(2,1)} custom-call(bf16[128,2048]{1,0:T(8,128)(2,1)} %rows.1, f32[1,2048]{1,0:T(1,128)} %bitcast.5, s32[4,128]{1,0:T(4,128)} %bitcast.8, f32[4,128]{1,0:T(4,128)} %bitcast.9), custom_call_target="tpu_custom_call" | custom-call | tf_op jit(solution)/shard_map/tokens/pallas_call | solution.py:295
  9.2 2.6 %collective-permute-start.17 = (bf16[64,2176]{1,0:T(8,128)(2,1)}, bf16[64,2176]{1,0:T(8,128)(2,1)S(1)}, u32[]{:S(2)}, u32[]{:S(2)}) collective-permute-start(bf16[64,2176]{1,0:T(8,128)(2,1)} %tokens.1.upper), channel_id=1, source_target_pairs={{0,16},{4,20},{8,24},{12,28},{16,0},{20,4},{24,8},{28,12},{1,17},{... | collective-permute-start | bytes 835592 | tf_op jit(solution)/shard_map/ppermute | solution.py:37
  12.2 1.3 %collective-permute-start.27 = (bf16[64,2176]{1,0:T(8,128)(2,1)}, bf16[64,2176]{1,0:T(8,128)(2,1)S(1)}, u32[]{:S(2)}, u32[]{:S(2)}) collective-permute-start(bf16[64,2176]{1,0:T(8,128)(2,1)} %tokens.1.upper), channel_id=1, source_target_pairs={{0,24},{4,28},{8,16},{12,20},{16,8},{20,12},{24,0},{28,4},{1,25},{... | collective-permute-start | bytes 835592 | tf_op jit(solution)/shard_map/ppermute | solution.py:37
  13.5 1.7 %collective-permute-start.1 = (bf16[64,640]{1,0:T(8,128)(2,1)}, bf16[64,640]{1,0:T(8,128)(2,1)S(1)}, u32[]{:S(2)}, u32[]{:S(2)}) collective-permute-start(bf16[64,640]{1,0:T(8,128)(2,1)} %keys.1), channel_id=1, source_target_pairs={{0,16},{4,20},{8,24},{12,28},{16,0},{20,4},{24,8},{28,12},{1,17},{... | collective-permute-start | bytes 245768 | tf_op jit(solution)/shard_map/ppermute | solution.py:37
  16.1 25.5 %collective-permute-done.1 = bf16[64,640]{1,0:T(8,128)(2,1)S(1)} collective-permute-done((bf16[64,640]{1,0:T(8,128)(2,1)}, bf16[64,640]{1,0:T(8,128)(2,1)S(1)}, u32[]{:S(2)}, u32[]{:S(2)}) %collective-permute-start.1) | collective-permute-done | bytes 81952 | tf_op jit(solution)/shard_map/ppermute | solution.py:37
  43.0 1.6 %collective-permute-start.3 = (bf16[256,640]{1,0:T(8,128)(2,1)S(1)}, bf16[256,640]{1,0:T(8,128)(2,1)S(1)}, u32[]{:S(2)}, u32[]{:S(2)}) collective-permute-start(bf16[256,640]{1,0:T(8,128)(2,1)S(1)} %pad_maximum_fusion.refs_0_), channel_id=1, source_target_pairs={{0,4},{4,0},{8,12},{12,8},{16,20},{20,16},{24,28},{28,24},{1,5},{5... | collective-permute-start | bytes 983048 | tf_op jit(solution)/shard_map/ppermute | solution.py:37
  45.2 8.5 %collective-permute-done.3.refs_1_ = bf16[256,640]{1,0:T(8,128)(2,1)S(1)} collective-permute-done((bf16[256,640]{1,0:T(8,128)(2,1)S(1)}, bf16[256,640]{1,0:T(8,128)(2,1)S(1)}, u32[]{:S(2)}, u32[]{:S(2)}) %collective-permute-start.3) | collective-permute-done | bytes 327712 | tf_op jit(solution)/shard_map/ppermute | solution.py:37
  53.7 5.0 %collective-permute-done.8.lower = bf16[64,2176]{1,0:T(8,128)(2,1)S(1)} collective-permute-done((bf16[64,2176]{1,0:T(8,128)(2,1)S(1)}, bf16[64,2176]{1,0:T(8,128)(2,1)S(1)}, u32[]{:S(2)}, u32[]{:S(2)}) %collective-permute-start.8) | collective-permute-done | bytes 278560 | tf_op jit(solution)/shard_map/ppermute | solution.py:37
  59.4 1.6 %collective-permute-start.18 = (bf16[64,2176]{1,0:T(8,128)(2,1)S(1)}, bf16[64,2176]{1,0:T(8,128)(2,1)S(1)}, u32[]{:S(2)}, u32[]{:S(2)}) collective-permute-start(bf16[64,2176]{1,0:T(8,128)(2,1)S(1)} %collective-permute-done.17.upper), channel_id=1, source_target_pairs={{0,4},{4,0},{8,12},{12,8},{16,20},{20,16},{24,28},{28,24},{1,5},{5... | collective-permute-start | bytes 835592 | tf_op jit(solution)/shard_map/ppermute | solution.py:37
  67.7 2.7 %attention.1 = (f32[64,2048]{1,0:T(8,128)S(1)}, bf16[64,2048]{1,0:T(8,128)(2,1)S(1)}) custom-call(bf16[128,640]{1,0:T(8,128)(2,1)S(1)} %queries.1, bf16[256,640]{1,0:T(8,128)(2,1)S(1)} %pad_maximum_fusion.refs_0_, bf16[256,640]{1,0:T(8,128)(2,1)S(1)} %collective-permute-done.3.refs_1_, bf16[256,640]{1,0:T(8,128)(2,1)S(1)} %collective-permute-done.4.refs_2_, ...), custom_call_target="tpu_custom_call" | custom-call | tf_op jit(solution)/shard_map/attention/pallas_call | solution.py:394
  70.5 3.9 %collective-permute-done.23.lower = bf16[64,2176]{1,0:T(8,128)(2,1)S(1)} collective-permute-done((bf16[64,2176]{1,0:T(8,128)(2,1)S(1)}, bf16[64,2176]{1,0:T(8,128)(2,1)S(1)}, u32[]{:S(2)}, u32[]{:S(2)}) %collective-permute-start.23) | collective-permute-done | bytes 278560 | tf_op jit(solution)/shard_map/ppermute | solution.py:37
  75.8 1.5 %collective-permute-start.28 = (bf16[64,2176]{1,0:T(8,128)(2,1)S(1)}, bf16[64,2176]{1,0:T(8,128)(2,1)S(1)}, u32[]{:S(2)}, u32[]{:S(2)}) collective-permute-start(bf16[64,2176]{1,0:T(8,128)(2,1)S(1)} %collective-permute-done.27.upper), channel_id=1, source_target_pairs={{0,4},{4,0},{8,12},{12,8},{16,20},{20,16},{24,28},{28,24},{1,5},{5... | collective-permute-start | bytes 835592 | tf_op jit(solution)/shard_map/ppermute | solution.py:37
  78.7 1.6 %collective-permute-start.7 = (bf16[32,2048]{1,0:T(8,128)(2,1)}, bf16[32,2048]{1,0:T(8,128)(2,1)S(1)}, u32[]{:S(2)}, u32[]{:S(2)}) collective-permute-start(bf16[32,2048]{1,0:T(8,128)(2,1)} %add_convert_fusion.7), channel_id=1, source_target_pairs={{0,2},{1,3},{2,0},{3,1},{4,6},{5,7},{6,4},{7,5},{8,10},{9,11},{10,... | collective-permute-start | bytes 393224 | tf_op jit(solution)/shard_map/ppermute | solution.py:37
  80.2 1.9 %experts.5 = (f32[128,1024]{1,0:T(8,128)S(1)}, bf16[128,1024]{1,0:T(8,128)(2,1)}) custom-call(bf16[64,2176]{1,0:T(8,128)(2,1)S(1)} %collective-permute-done.17.upper, bf16[64,2176]{1,0:T(8,128)(2,1)S(1)} %collective-permute-done.18.lower, bf16[1,2048,256]{2,1,0:T(8,128)(2,1)S(1)} %collective-permute-done.9.refs_0_, ...), custom_call_target="tpu_custom_call" | custom-call | tf_op jit(solution)/shard_map/experts/pallas_call | solution.py:205
  83.0 1.8 %collective-permute-done.28.lower = bf16[64,2176]{1,0:T(8,128)(2,1)S(1)} collective-permute-done((bf16[64,2176]{1,0:T(8,128)(2,1)S(1)}, bf16[64,2176]{1,0:T(8,128)(2,1)S(1)}, u32[]{:S(2)}, u32[]{:S(2)}) %collective-permute-start.28) | collective-permute-done | bytes 278560 | tf_op jit(solution)/shard_map/ppermute | solution.py:37
  85.5 1.5 %collective-permute-start.19 = (bf16[128,1024]{1,0:T(8,128)(2,1)}, bf16[128,1024]{1,0:T(8,128)(2,1)}, u32[]{:S(2)}, u32[]{:S(2)}) collective-permute-start(bf16[128,1024]{1,0:T(8,128)(2,1)} %get-tuple-element.17), channel_id=1, source_target_pairs={{0,2},{1,3},{2,0},{3,1},{4,6},{5,7},{6,4},{7,5},{8,10},{9,11},{10,... | collective-permute-start | bytes 786440 | tf_op jit(solution)/shard_map/ppermute | solution.py:37
  87.0 1.2 copy-done.4
  88.2 1.2 copy-done.7
  89.4 1.2 copy-done.9
  96.0 1.5 %collective-permute-start.29 = (bf16[128,1024]{1,0:T(8,128)(2,1)S(1)}, bf16[128,1024]{1,0:T(8,128)(2,1)S(1)}, u32[]{:S(2)}, u32[]{:S(2)}) collective-permute-start(bf16[128,1024]{1,0:T(8,128)(2,1)S(1)} %get-tuple-element.21), channel_id=1, source_target_pairs={{0,2},{1,3},{2,0},{3,1},{4,6},{5,7},{6,4},{7,5},{8,10},{9,11},{10,... | collective-permute-start | bytes 786440 | tf_op jit(solution)/shard_map/ppermute | solution.py:37
  97.5 3.9 %experts.4 = (f32[128,1024]{1,0:T(8,128)S(1)}, bf16[128,1024]{1,0:T(8,128)(2,1)S(1)}) custom-call(bf16[64,2176]{1,0:T(8,128)(2,1)S(1)} %copy-done.13, bf16[64,2176]{1,0:T(8,128)(2,1)S(1)} %copy-done.23, bf16[1,2048,256]{2,1,0:T(8,128)(2,1)S(1)} %copy-done.10, bf16[1,2048,256]{2,1,0:T(8,128)(2,1)S(1)} %copy-done.5, bf16[1,256,2048]{2,1,0:T(8,128)(2,1)S(1)} %copy-done.7, ...), custom_call_target="tpu_custom_call" | custom-call | tf_op jit(solution)/shard_map/experts/pallas_call | solution.py:205
  103.4 1.6 %collective-permute-start.20 = (bf16[64,1024]{1,0:T(8,128)(2,1)S(1)}, bf16[64,1024]{1,0:T(8,128)(2,1)S(1)}, u32[]{:S(2)}, u32[]{:S(2)}) collective-permute-start(bf16[64,1024]{1,0:T(8,128)(2,1)S(1)} %add_convert_fusion.5), channel_id=1, source_target_pairs={{0,4},{4,0},{8,12},{12,8},{16,20},{20,16},{24,28},{28,24},{1,5},{5... | collective-permute-start | bytes 393224 | tf_op jit(solution)/shard_map/ppermute | solution.py:37
  105.0 1.3 collective-permute-start.25
  106.3 4.0 %collective-permute-done.29 = bf16[128,1024]{1,0:T(8,128)(2,1)S(1)} collective-permute-done((bf16[128,1024]{1,0:T(8,128)(2,1)S(1)}, bf16[128,1024]{1,0:T(8,128)(2,1)S(1)}, u32[]{:S(2)}, u32[]{:S(2)}) %collective-permute-start.29) | collective-permute-done | bytes 262176 | tf_op jit(solution)/shard_map/ppermute | solution.py:37
  110.3 1.6 %collective-permute-start.30 = (bf16[64,1024]{1,0:T(8,128)(2,1)S(1)}, bf16[64,1024]{1,0:T(8,128)(2,1)S(1)}, u32[]{:S(2)}, u32[]{:S(2)}) collective-permute-start(bf16[64,1024]{1,0:T(8,128)(2,1)S(1)} %add_convert_fusion.1), channel_id=1, source_target_pairs={{0,4},{4,0},{8,12},{12,8},{16,20},{20,16},{24,28},{28,24},{1,5},{5... | collective-permute-start | bytes 393224 | tf_op jit(solution)/shard_map/ppermute | solution.py:37
  111.9 2.3 %collective-permute-done.15 = bf16[128,1024]{1,0:T(8,128)(2,1)S(1)} collective-permute-done((bf16[128,1024]{1,0:T(8,128)(2,1)S(1)}, bf16[128,1024]{1,0:T(8,128)(2,1)S(1)}, u32[]{:S(2)}, u32[]{:S(2)}) %collective-permute-start.15) | collective-permute-done | bytes 262176 | tf_op jit(solution)/shard_map/ppermute | solution.py:37
  114.3 1.6 %collective-permute-start.16 = (bf16[64,1024]{1,0:T(8,128)(2,1)S(1)}, bf16[64,1024]{1,0:T(8,128)(2,1)S(1)}, u32[]{:S(2)}, u32[]{:S(2)}) collective-permute-start(bf16[64,1024]{1,0:T(8,128)(2,1)S(1)} %add_convert_fusion.6), channel_id=1, source_target_pairs={{0,4},{4,0},{8,12},{12,8},{16,20},{20,16},{24,28},{28,24},{1,5},{5... | collective-permute-start | bytes 393224 | tf_op jit(solution)/shard_map/ppermute | solution.py:37
  116.8 3.4 %collective-permute-start.21 = (bf16[64,1024]{1,0:T(8,128)(2,1)S(1)}, bf16[64,1024]{1,0:T(8,128)(2,1)S(1)}, u32[]{:S(2)}, u32[]{:S(2)}) collective-permute-start(bf16[64,1024]{1,0:T(8,128)(2,1)S(1)} %add_convert_fusion.4), channel_id=1, source_target_pairs={{0,16},{4,20},{8,24},{12,28},{16,0},{20,4},{24,8},{28,12},{1,17},{... | collective-permute-start | bytes 393224 | tf_op jit(solution)/shard_map/ppermute | solution.py:37
  121.9 5.4 %collective-permute-done.21 = bf16[64,1024]{1,0:T(8,128)(2,1)S(1)} collective-permute-done((bf16[64,1024]{1,0:T(8,128)(2,1)S(1)}, bf16[64,1024]{1,0:T(8,128)(2,1)S(1)}, u32[]{:S(2)}, u32[]{:S(2)}) %collective-permute-start.21) | collective-permute-done | bytes 131104 | tf_op jit(solution)/shard_map/ppermute | solution.py:37
  127.4 1.4 %collective-permute-done.31 = bf16[64,1024]{1,0:T(8,128)(2,1)S(1)} collective-permute-done((bf16[64,1024]{1,0:T(8,128)(2,1)S(1)}, bf16[64,1024]{1,0:T(8,128)(2,1)S(1)}, u32[]{:S(2)}, u32[]{:S(2)}) %collective-permute-start.31) | collective-permute-done | bytes 131104 | tf_op jit(solution)/shard_map/ppermute | solution.py:37
  (135 shorter events, 29.0 us)
Async XLA Ops:
  4.1 11.2 %collective-permute-start = (bf16[64,640]{1,0:T(8,128)(2,1)}, bf16[64,640]{1,0:T(8,128)(2,1)S(1)}, u32[]{:S(2)}, u32[]{:S(2)}) collective-permute-start(bf16[64,640]{1,0:T(8,128)(2,1)} %keys.1), channel_id=1, source_target_pairs={{0,8},{4,12},{8,0},{12,4},{16,24},{20,28},{24,16},{28,20},{1,9},{5... | collective-permute-start | bytes 245768 | tf_op jit(solution)/shard_map/ppermute | solution.py:37
  9.2 33.9 %collective-permute-start.17 = (bf16[64,2176]{1,0:T(8,128)(2,1)}, bf16[64,2176]{1,0:T(8,128)(2,1)S(1)}, u32[]{:S(2)}, u32[]{:S(2)}) collective-permute-start(bf16[64,2176]{1,0:T(8,128)(2,1)} %tokens.1.upper), channel_id=1, source_target_pairs={{0,16},{4,20},{8,24},{12,28},{16,0},{20,4},{24,8},{28,12},{1,17},{... | collective-permute-start | bytes 835592 | tf_op jit(solution)/shard_map/ppermute | solution.py:37
  11.7 32.9 %collective-permute-start.22 = (bf16[64,2176]{1,0:T(8,128)(2,1)}, bf16[64,2176]{1,0:T(8,128)(2,1)S(1)}, u32[]{:S(2)}, u32[]{:S(2)}) collective-permute-start(bf16[64,2176]{1,0:T(8,128)(2,1)} %tokens.1.upper), channel_id=1, source_target_pairs={{0,8},{4,12},{8,0},{12,4},{16,24},{20,28},{24,16},{28,20},{1,9},{5... | collective-permute-start | bytes 835592 | tf_op jit(solution)/shard_map/ppermute | solution.py:37
  12.2 32.4 %collective-permute-start.27 = (bf16[64,2176]{1,0:T(8,128)(2,1)}, bf16[64,2176]{1,0:T(8,128)(2,1)S(1)}, u32[]{:S(2)}, u32[]{:S(2)}) collective-permute-start(bf16[64,2176]{1,0:T(8,128)(2,1)} %tokens.1.upper), channel_id=1, source_target_pairs={{0,24},{4,28},{8,16},{12,20},{16,8},{20,12},{24,0},{28,4},{1,25},{... | collective-permute-start | bytes 835592 | tf_op jit(solution)/shard_map/ppermute | solution.py:37
  13.5 28.1 %collective-permute-start.1 = (bf16[64,640]{1,0:T(8,128)(2,1)}, bf16[64,640]{1,0:T(8,128)(2,1)S(1)}, u32[]{:S(2)}, u32[]{:S(2)}) collective-permute-start(bf16[64,640]{1,0:T(8,128)(2,1)} %keys.1), channel_id=1, source_target_pairs={{0,16},{4,20},{8,24},{12,28},{16,0},{20,4},{24,8},{28,12},{1,17},{... | collective-permute-start | bytes 245768 | tf_op jit(solution)/shard_map/ppermute | solution.py:37
  15.2 26.4 %collective-permute-start.2 = (bf16[64,640]{1,0:T(8,128)(2,1)}, bf16[64,640]{1,0:T(8,128)(2,1)S(1)}, u32[]{:S(2)}, u32[]{:S(2)}) collective-permute-start(bf16[64,640]{1,0:T(8,128)(2,1)} %keys.1), channel_id=1, source_target_pairs={{0,24},{4,28},{8,16},{12,20},{16,8},{20,12},{24,0},{28,4},{1,25},{... | collective-permute-start | bytes 245768 | tf_op jit(solution)/shard_map/ppermute | solution.py:37
  41.6 34.1 %collective-permute-start.10 = (bf16[1,2048,256]{2,1,0:T(8,128)(2,1)}, bf16[1,2048,256]{2,1,0:T(8,128)(2,1)S(1)}, u32[]{:S(2)}, u32[]{:S(2)}) collective-permute-start(bf16[1,2048,256]{2,1,0:T(8,128)(2,1)} %refs_4_.9), channel_id=1, source_target_pairs={{0,1},{1,0},{2,3},{3,2},{4,5},{5,4},{6,7},{7,6},{8,9},{9,8},{10,11... | collective-permute-start | bytes 3145736 | tf_op jit(solution)/shard_map/ppermute | solution.py:37
  41.6 34.1 %collective-permute-start.11 = (bf16[1,256,2048]{2,1,0:T(8,128)(2,1)}, bf16[1,256,2048]{2,1,0:T(8,128)(2,1)S(1)}, u32[]{:S(2)}, u32[]{:S(2)}) collective-permute-start(bf16[1,256,2048]{2,1,0:T(8,128)(2,1)} %refs_5_.9), channel_id=1, source_target_pairs={{0,1},{1,0},{2,3},{3,2},{4,5},{5,4},{6,7},{7,6},{8,9},{9,8},{10,11... | collective-permute-start | bytes 3145736 | tf_op jit(solution)/shard_map/ppermute | solution.py:37
  43.0 10.7 %collective-permute-start.3 = (bf16[256,640]{1,0:T(8,128)(2,1)S(1)}, bf16[256,640]{1,0:T(8,128)(2,1)S(1)}, u32[]{:S(2)}, u32[]{:S(2)}) collective-permute-start(bf16[256,640]{1,0:T(8,128)(2,1)S(1)} %pad_maximum_fusion.refs_0_), channel_id=1, source_target_pairs={{0,4},{4,0},{8,12},{12,8},{16,20},{20,16},{24,28},{28,24},{1,5},{5... | collective-permute-start | bytes 983048 | tf_op jit(solution)/shard_map/ppermute | solution.py:37
  44.6 14.8 %collective-permute-start.4 = (bf16[256,640]{1,0:T(8,128)(2,1)S(1)}, bf16[256,640]{1,0:T(8,128)(2,1)S(1)}, u32[]{:S(2)}, u32[]{:S(2)}) collective-permute-start(bf16[256,640]{1,0:T(8,128)(2,1)S(1)} %pad_maximum_fusion.refs_0_), channel_id=1, source_target_pairs={{0,1},{1,0},{2,3},{3,2},{4,5},{5,4},{6,7},{7,6},{8,9},{9,8},{10,11... | collective-permute-start | bytes 983048 | tf_op jit(solution)/shard_map/ppermute | solution.py:37
  44.6 14.1 %collective-permute-start.8 = (bf16[64,2176]{1,0:T(8,128)(2,1)S(1)}, bf16[64,2176]{1,0:T(8,128)(2,1)S(1)}, u32[]{:S(2)}, u32[]{:S(2)}) collective-permute-start(bf16[64,2176]{1,0:T(8,128)(2,1)S(1)} %copy-done.13), channel_id=1, source_target_pairs={{0,4},{4,0},{8,12},{12,8},{16,20},{20,16},{24,28},{28,24},{1,5},{5... | collective-permute-start | bytes 835592 | tf_op jit(solution)/shard_map/ppermute | solution.py:37
  53.7 7.3 %collective-permute-start.5 = (bf16[256,640]{1,0:T(8,128)(2,1)S(1)}, bf16[256,640]{1,0:T(8,128)(2,1)S(1)}, u32[]{:S(2)}, u32[]{:S(2)}) collective-permute-start(bf16[256,640]{1,0:T(8,128)(2,1)S(1)} %collective-permute-done.3.refs_1_), channel_id=1, source_target_pairs={{0,1},{1,0},{2,3},{3,2},{4,5},{5,4},{6,7},{7,6},{8,9},{9,8},{10,11... | collective-permute-start | bytes 983048 | tf_op jit(solution)/shard_map/ppermute | solution.py:37
  59.4 19.3 %collective-permute-start.9 = (bf16[1,2048,256]{2,1,0:T(8,128)(2,1)S(1)}, bf16[1,2048,256]{2,1,0:T(8,128)(2,1)S(1)}, u32[]{:S(2)}, u32[]{:S(2)}) collective-permute-start(bf16[1,2048,256]{2,1,0:T(8,128)(2,1)S(1)} %copy-done), channel_id=1, source_target_pairs={{0,1},{1,0},{2,3},{3,2},{4,5},{5,4},{6,7},{7,6},{8,9},{9,8},{10,11... | collective-permute-start | bytes 3145736 | tf_op jit(solution)/shard_map/ppermute | solution.py:37
  59.4 11.0 %collective-permute-start.18 = (bf16[64,2176]{1,0:T(8,128)(2,1)S(1)}, bf16[64,2176]{1,0:T(8,128)(2,1)S(1)}, u32[]{:S(2)}, u32[]{:S(2)}) collective-permute-start(bf16[64,2176]{1,0:T(8,128)(2,1)S(1)} %collective-permute-done.17.upper), channel_id=1, source_target_pairs={{0,4},{4,0},{8,12},{12,8},{16,20},{20,16},{24,28},{28,24},{1,5},{5... | collective-permute-start | bytes 835592 | tf_op jit(solution)/shard_map/ppermute | solution.py:37
  61.0 13.5 %collective-permute-start.23 = (bf16[64,2176]{1,0:T(8,128)(2,1)S(1)}, bf16[64,2176]{1,0:T(8,128)(2,1)S(1)}, u32[]{:S(2)}, u32[]{:S(2)}) collective-permute-start(bf16[64,2176]{1,0:T(8,128)(2,1)S(1)} %collective-permute-done.22.upper), channel_id=1, source_target_pairs={{0,4},{4,0},{8,12},{12,8},{16,20},{20,16},{24,28},{28,24},{1,5},{5... | collective-permute-start | bytes 835592 | tf_op jit(solution)/shard_map/ppermute | solution.py:37
  70.5 4.7 %collective-permute-start.6 = (bf16[64,2048]{1,0:T(8,128)(2,1)S(1)}, bf16[64,2048]{1,0:T(8,128)(2,1)S(1)}, u32[]{:S(2)}, u32[]{:S(2)}) collective-permute-start(bf16[64,2048]{1,0:T(8,128)(2,1)S(1)} %get-tuple-element.13), channel_id=1, source_target_pairs={{0,1},{1,0},{2,3},{3,2},{4,5},{5,4},{6,7},{7,6},{8,9},{9,8},{10,11... | collective-permute-start | bytes 786440 | tf_op jit(solution)/shard_map/ppermute | solution.py:37
  75.1 20.3 %collective-permute-start.12 = (bf16[2048,128]{1,0:T(8,128)(2,1)}, bf16[2048,128]{1,0:T(8,128)(2,1)}, u32[]{:S(2)}, u32[]{:S(2)}) collective-permute-start(bf16[2048,128]{1,0:T(8,128)(2,1)} %refs_3_.4), channel_id=1, source_target_pairs={{0,1},{1,0},{2,3},{3,2},{4,5},{5,4},{6,7},{7,6},{8,9},{9,8},{10,11... | collective-permute-start | bytes 1572872 | tf_op jit(solution)/shard_map/ppermute | solution.py:37
  75.2 20.9 %collective-permute-start.13 = (bf16[2048,128]{1,0:T(8,128)(2,1)}, bf16[2048,128]{1,0:T(8,128)(2,1)}, u32[]{:S(2)}, u32[]{:S(2)}) collective-permute-start(bf16[2048,128]{1,0:T(8,128)(2,1)} %refs_4_.6), channel_id=1, source_target_pairs={{0,1},{1,0},{2,3},{3,2},{4,5},{5,4},{6,7},{7,6},{8,9},{9,8},{10,11... | collective-permute-start | bytes 1572872 | tf_op jit(solution)/shard_map/ppermute | solution.py:37
  75.7 21.9 %collective-permute-start.14 = (bf16[128,2048]{1,0:T(8,128)(2,1)}, bf16[128,2048]{1,0:T(8,128)(2,1)}, u32[]{:S(2)}, u32[]{:S(2)}) collective-permute-start(bf16[128,2048]{1,0:T(8,128)(2,1)} %refs_5_.6), channel_id=1, source_target_pairs={{0,1},{1,0},{2,3},{3,2},{4,5},{5,4},{6,7},{7,6},{8,9},{9,8},{10,11... | collective-permute-start | bytes 1572872 | tf_op jit(solution)/shard_map/ppermute | solution.py:37
  75.8 9.0 %collective-permute-start.28 = (bf16[64,2176]{1,0:T(8,128)(2,1)S(1)}, bf16[64,2176]{1,0:T(8,128)(2,1)S(1)}, u32[]{:S(2)}, u32[]{:S(2)}) collective-permute-start(bf16[64,2176]{1,0:T(8,128)(2,1)S(1)} %collective-permute-done.27.upper), channel_id=1, source_target_pairs={{0,4},{4,0},{8,12},{12,8},{16,20},{20,16},{24,28},{28,24},{1,5},{5... | collective-permute-start | bytes 835592 | tf_op jit(solution)/shard_map/ppermute | solution.py:37
  78.7 23.3 %collective-permute-start.7 = (bf16[32,2048]{1,0:T(8,128)(2,1)}, bf16[32,2048]{1,0:T(8,128)(2,1)S(1)}, u32[]{:S(2)}, u32[]{:S(2)}) collective-permute-start(bf16[32,2048]{1,0:T(8,128)(2,1)} %add_convert_fusion.7), channel_id=1, source_target_pairs={{0,2},{1,3},{2,0},{3,1},{4,6},{5,7},{6,4},{7,5},{8,10},{9,11},{10,... | collective-permute-start | bytes 393224 | tf_op jit(solution)/shard_map/ppermute | solution.py:37
  85.5 16.7 %collective-permute-start.19 = (bf16[128,1024]{1,0:T(8,128)(2,1)}, bf16[128,1024]{1,0:T(8,128)(2,1)}, u32[]{:S(2)}, u32[]{:S(2)}) collective-permute-start(bf16[128,1024]{1,0:T(8,128)(2,1)} %get-tuple-element.17), channel_id=1, source_target_pairs={{0,2},{1,3},{2,0},{3,1},{4,6},{5,7},{6,4},{7,5},{8,10},{9,11},{10,... | collective-permute-start | bytes 786440 | tf_op jit(solution)/shard_map/ppermute | solution.py:37
  95.4 9.5 %collective-permute-start.24 = (bf16[128,1024]{1,0:T(8,128)(2,1)S(1)}, bf16[128,1024]{1,0:T(8,128)(2,1)S(1)}, u32[]{:S(2)}, u32[]{:S(2)}) collective-permute-start(bf16[128,1024]{1,0:T(8,128)(2,1)S(1)} %get-tuple-element.19), channel_id=1, source_target_pairs={{0,2},{1,3},{2,0},{3,1},{4,6},{5,7},{6,4},{7,5},{8,10},{9,11},{10,... | collective-permute-start | bytes 786440 | tf_op jit(solution)/shard_map/ppermute | solution.py:37
  96.0 14.2 %collective-permute-start.29 = (bf16[128,1024]{1,0:T(8,128)(2,1)S(1)}, bf16[128,1024]{1,0:T(8,128)(2,1)S(1)}, u32[]{:S(2)}, u32[]{:S(2)}) collective-permute-start(bf16[128,1024]{1,0:T(8,128)(2,1)S(1)} %get-tuple-element.21), channel_id=1, source_target_pairs={{0,2},{1,3},{2,0},{3,1},{4,6},{5,7},{6,4},{7,5},{8,10},{9,11},{10,... | collective-permute-start | bytes 786440 | tf_op jit(solution)/shard_map/ppermute | solution.py:37
  101.4 12.8 %collective-permute-start.15 = (bf16[128,1024]{1,0:T(8,128)(2,1)S(1)}, bf16[128,1024]{1,0:T(8,128)(2,1)S(1)}, u32[]{:S(2)}, u32[]{:S(2)}) collective-permute-start(bf16[128,1024]{1,0:T(8,128)(2,1)S(1)} %get-tuple-element.15), channel_id=1, source_target_pairs={{0,2},{1,3},{2,0},{3,1},{4,6},{5,7},{6,4},{7,5},{8,10},{9,11},{10,... | collective-permute-start | bytes 786440 | tf_op jit(solution)/shard_map/ppermute | solution.py:37
  103.4 12.5 %collective-permute-start.20 = (bf16[64,1024]{1,0:T(8,128)(2,1)S(1)}, bf16[64,1024]{1,0:T(8,128)(2,1)S(1)}, u32[]{:S(2)}, u32[]{:S(2)}) collective-permute-start(bf16[64,1024]{1,0:T(8,128)(2,1)S(1)} %add_convert_fusion.5), channel_id=1, source_target_pairs={{0,4},{4,0},{8,12},{12,8},{16,20},{20,16},{24,28},{28,24},{1,5},{5... | collective-permute-start | bytes 393224 | tf_op jit(solution)/shard_map/ppermute | solution.py:37
  105.0 15.2 %collective-permute-start.25 = (bf16[64,1024]{1,0:T(8,128)(2,1)S(1)}, bf16[64,1024]{1,0:T(8,128)(2,1)S(1)}, u32[]{:S(2)}, u32[]{:S(2)}) collective-permute-start(bf16[64,1024]{1,0:T(8,128)(2,1)S(1)} %add_convert_fusion.3), channel_id=1, source_target_pairs={{0,4},{4,0},{8,12},{12,8},{16,20},{20,16},{24,28},{28,24},{1,5},{5... | collective-permute-start | bytes 393224 | tf_op jit(solution)/shard_map/ppermute | solution.py:37
  110.3 10.6 %collective-permute-start.30 = (bf16[64,1024]{1,0:T(8,128)(2,1)S(1)}, bf16[64,1024]{1,0:T(8,128)(2,1)S(1)}, u32[]{:S(2)}, u32[]{:S(2)}) collective-permute-start(bf16[64,1024]{1,0:T(8,128)(2,1)S(1)} %add_convert_fusion.1), channel_id=1, source_target_pairs={{0,4},{4,0},{8,12},{12,8},{16,20},{20,16},{24,28},{28,24},{1,5},{5... | collective-permute-start | bytes 393224 | tf_op jit(solution)/shard_map/ppermute | solution.py:37
  114.3 7.7 %collective-permute-start.16 = (bf16[64,1024]{1,0:T(8,128)(2,1)S(1)}, bf16[64,1024]{1,0:T(8,128)(2,1)S(1)}, u32[]{:S(2)}, u32[]{:S(2)}) collective-permute-start(bf16[64,1024]{1,0:T(8,128)(2,1)S(1)} %add_convert_fusion.6), channel_id=1, source_target_pairs={{0,4},{4,0},{8,12},{12,8},{16,20},{20,16},{24,28},{28,24},{1,5},{5... | collective-permute-start | bytes 393224 | tf_op jit(solution)/shard_map/ppermute | solution.py:37
  116.8 10.6 %collective-permute-start.21 = (bf16[64,1024]{1,0:T(8,128)(2,1)S(1)}, bf16[64,1024]{1,0:T(8,128)(2,1)S(1)}, u32[]{:S(2)}, u32[]{:S(2)}) collective-permute-start(bf16[64,1024]{1,0:T(8,128)(2,1)S(1)} %add_convert_fusion.4), channel_id=1, source_target_pairs={{0,16},{4,20},{8,24},{12,28},{16,0},{20,4},{24,8},{28,12},{1,17},{... | collective-permute-start | bytes 393224 | tf_op jit(solution)/shard_map/ppermute | solution.py:37
  120.2 7.1 %collective-permute-start.26 = (bf16[64,1024]{1,0:T(8,128)(2,1)S(1)}, bf16[64,1024]{1,0:T(8,128)(2,1)S(1)}, u32[]{:S(2)}, u32[]{:S(2)}) collective-permute-start(bf16[64,1024]{1,0:T(8,128)(2,1)S(1)} %add_convert_fusion.2), channel_id=1, source_target_pairs={{0,8},{4,12},{8,0},{12,4},{16,24},{20,28},{24,16},{28,20},{1,9},{5... | collective-permute-start | bytes 393224 | tf_op jit(solution)/shard_map/ppermute | solution.py:37
  121.0 7.8 %collective-permute-start.31 = (bf16[64,1024]{1,0:T(8,128)(2,1)S(1)}, bf16[64,1024]{1,0:T(8,128)(2,1)S(1)}, u32[]{:S(2)}, u32[]{:S(2)}) collective-permute-start(bf16[64,1024]{1,0:T(8,128)(2,1)S(1)} %add_convert_fusion), channel_id=1, source_target_pairs={{0,24},{4,28},{8,16},{12,20},{16,8},{20,12},{24,0},{28,4},{1,25},{... | collective-permute-start | bytes 393224 | tf_op jit(solution)/shard_map/ppermute | solution.py:37
  (38 other events, 304.9 us)
where the time goes:
time: 132 us; the launch traced here: 131 us
  waiting for transfers between devices  57.9 us (44%)
  starting transfers between devices  33.8 us (26%)
  local copies, waits for them, and re-layouts  16.3 us (12%)
  Pallas kernels  15.8 us (12%)
  other arithmetic  6.32 us (5%)
    ppermute x33, waiting for transfers between devices, swap(): return lax.ppermute(values, axis, [(i, i ^ mask) for i in range(count)])  57.9 us
    ppermute x33, starting transfers between devices, swap(): return lax.ppermute(values, axis, [(i, i ^ mask) for i in range(count)])  33.8 us
    unnamed x74, local copies, waits for them, and re-layouts  15.6 us
    pallas_call x4, Pallas kernels, call_experts(): pl.pallas_call(functools.partial(expert_kernel, held_count=len(held), str...  8.13 us
    pallas_call x1, Pallas kernels, per_device(): pl.pallas_call(functools.partial(attention_kernel, head_count=head_count,...  2.72 us
  transfers between devices with their start and end apart: 33, of which 9 were waited for; matrix products, arithmetic and copies ran while one was open for 4% of the time, Pallas kernels for 11%

commit v1 on v0

--- a/solution.py
+++ b/solution.py
@@ -22,6 +22,10 @@
 MIB = 2**20
 
 
+def far_off(values):
+    return pltpu.with_memory_space_constraint(values, pltpu.HBM)
+
+
 def within(mib):
     return pltpu.CompilerParams(vmem_limit_bytes=mib * MIB)
 
@@ -48,6 +52,17 @@
 def gated(rows, gate, up):
     gate_act = dot32(rows, gate)
     return gate_act / (1.0 + jnp.exp(-gate_act)) * dot32(rows, up)
+
+
+def angles_of(block, width):
+    place = lax.broadcasted_iota(jnp.int32, (block, width), 0) + lax.axis_index("ep") * block
+    return place.astype(jnp.float32)
+
+
+def inverses(width):
+    pair = np.arange(width) % (ROPE // 2)
+    power = np.float32(ROPE_BASE) ** (pair.astype(np.float32) * np.float32(2.0 / ROPE))
+    return (np.float32(1.0) / power).astype(np.float32).reshape(1, width)
 
 
 def token_kernel(rows, gain, ids, weights, out, table, *, expert_count):
@@ -66,30 +81,63 @@
     out[:, width:] = table[pl.ds(start, half), :].astype(jnp.bfloat16)
 
 
-def key_kernel(latent, gain, rotary, cosine, sine, spread, out, both):
+def key_kernel(latent, gain, rotary, spread, inverse, out, both):
     half = out.shape[0]
     width = latent.shape[1]
+    turned = inverse.shape[1]
     start = pl.multiple_of(lax.axis_index("tp") % 2 * half, half)
     out[:, :width] = rms_scale(latent[pl.ds(start, half), :], gain[...])
-    both[...] = lax.dot_general(
+    copied = lax.dot_general(
         rotary[...], spread[...], (((0,), (0,)), ((), ())), preferred_element_type=jnp.float32
     )
-    turned = both.shape[1] // 2
-    out[:, width:] = (
-        both[pl.ds(start, half), :turned] * cosine[pl.ds(start, half), :]
-        + both[pl.ds(start, half), turned:] * sine[pl.ds(start, half), :]
-    ).astype(jnp.bfloat16)
-
-
-def query_kernel(latent, gain, weight, order, cosine, sine, out):
-    turned = cosine.shape[1]
+    angle = angles_of(latent.shape[0], turned) * inverse[...]
+    both[...] = copied[:, :turned] * jnp.cos(angle) + copied[:, turned:] * jnp.sin(angle)
+    out[:, width:] = both[pl.ds(start, half), :].astype(jnp.bfloat16)
+
+
+def hold_kernel(*refs):
+    count = len(refs) // 2
+    hbm, landed, sems = refs[:count], refs[count : 2 * count], refs[-1]
+    copies = [pltpu.make_async_copy(hbm[i], landed[i], sems.at[i]) for i in range(count)]
+    for copy in copies:
+        copy.start()
+    for copy in copies:
+        copy.wait()
+
+
+def query_kernel(latent, gain, weight, order, inverse, out):
+    turned = inverse.shape[1]
     plain = out.shape[1] - turned
     ordered = dot32(weight[...], order[...]).astype(jnp.bfloat16)
     both = dot32(rms_scale(latent[...], gain[...]), ordered)
     out[:, :plain] = both[:, :plain].astype(jnp.bfloat16)
+    angle = angles_of(latent.shape[0], turned) * inverse[...]
     out[:, plain:] = (
-        both[:, plain : plain + turned] * cosine[...] + both[:, plain + turned :] * sine[...]
+        both[:, plain : plain + turned] * jnp.cos(angle)
+        + both[:, plain + turned :] * jnp.sin(angle)
     ).astype(jnp.bfloat16)
+
+
+def sum_kernel(own, *refs):
+    parts = refs[:-3]
+    mine, other, total = refs[-3:]
+    value = own[...]
+    for part in parts:
+        value = value + part[...].astype(jnp.float32)
+    total[...] = value
+    column = mine.shape[1]
+    core = lax.axis_index("tp") % 2
+    mine[...] = total[:, pl.ds(pl.multiple_of(core * column, column), column)].astype(jnp.bfloat16)
+    other[...] = total[:, pl.ds(pl.multiple_of((1 - core) * column, column), column)].astype(
+        jnp.bfloat16
+    )
+
+
+def join_kernel(mine, other, out):
+    half = mine.shape[0]
+    core = lax.axis_index("tp") % 2
+    out[pl.ds(pl.multiple_of(core * half, half), half), :] = mine[...]
+    out[pl.ds(pl.multiple_of((1 - core) * half, half), half), :] = other[...]
 
 
 def attention_kernel(queries, *refs, head_count, piece_count, tp_count):
@@ -143,50 +191,35 @@
         send[span, :] = part[pl.ds(there, quarter), :].astype(jnp.bfloat16)
 
 
-def expert_kernel(upper, lower, *refs, held_count, stream_count, expert_count):
-    held = refs[:held_count]
-    hbm = refs[held_count : held_count + stream_count]
-    keep, send, part = refs[held_count + stream_count : held_count + stream_count + 3]
-    copies = []
-    if stream_count:
-        sems = refs[-stream_count - 1]
-        landed = refs[-stream_count:]
-        copies = [
-            pltpu.make_async_copy(hbm[i], landed[i], sems.at[i]) for i in range(stream_count)
-        ]
-        for copy in copies:
-            copy.start()
-    half = upper.shape[0]
+def expert_kernel(*refs, unit_count, routed_count, shared_count, expert_count):
+    units = refs[:unit_count]
+    weights = refs[unit_count : unit_count + routed_count]
+    shared = refs[unit_count + routed_count : unit_count + routed_count + shared_count]
+    keep, send, part = refs[unit_count + routed_count + shared_count :]
+    half = units[0].shape[0]
     width = part.shape[1]
-    rows = jnp.concatenate([upper[:, :width], lower[:, :width]], 0)
-    scale = jnp.concatenate([upper[:, width:], lower[:, width:]], 0).astype(jnp.float32)
+    rows = jnp.concatenate([u[:, :width] for u in units], 0)
+    scale = jnp.concatenate([u[:, width:] for u in units], 0).astype(jnp.float32)
     spots = lax.broadcasted_iota(jnp.int32, scale.shape, 1)
-    local_count = held[0].shape[0]
-
-    def routed(gate, up, down):
-        total = None
-        for i in range(local_count):
-            mine = lax.axis_index("ep") * local_count + i
-            hot = (spots == mine) | (spots == mine + expert_count)
-            factor = jnp.sum(jnp.where(hot, scale, 0.0), 1, keepdims=True)
+    local_count = weights[0].shape[0]
+    total = None
+    for i in range(local_count):
+        mine = lax.axis_index("ep") * local_count + i
+        hot = (spots == mine) | (spots == mine + expert_count)
+        factor = jnp.sum(jnp.where(hot, scale, 0.0), 1, keepdims=True)
+        for at in range(0, routed_count, 3):
+            gate, up, down = weights[at : at + 3]
             hidden = (gated(rows, gate[i], up[i]) * factor).astype(jnp.bfloat16)
             term = dot32(hidden, down[i])
             total = term if total is None else total + term
-        return total
-
-    total = routed(*held[:3])
-    for at in range(3, held_count, 3):
-        total = total + routed(*held[at : at + 3])
     part[...] = total
-    for at in range(0, stream_count, 3):
-        for copy in copies[at : at + 3]:
-            copy.wait()
-        gate, up, down = landed[at : at + 3]
-        if at < stream_count - 3:
-            hidden = gated(rows[:half], gate[...], up[...]).astype(jnp.bfloat16)
-            part[:half, :] = part[:half, :] + dot32(hidden, down[...])
-        else:
-            part[...] = part[...] + routed(gate, up, down)
+    if shared_count:
+        gate, up, down = (
+            jnp.concatenate([shared[i][...], shared[i + 3][...]], 0 if i == 2 else 1)
+            for i in range(3)
+        )
+        hidden = gated(rows[:half], gate, up).astype(jnp.bfloat16)
+        part[:half, :] = part[:half, :] + dot32(hidden, down)
     column = keep.shape[1]
     side = lax.axis_index("tp") // 2
     here = pl.multiple_of(side * column, column)
@@ -195,30 +228,27 @@
     send[...] = part[:, pl.ds(there, column)].astype(jnp.bfloat16)
 
 
-def call_experts(upper, lower, held, streamed, model_width, expert_count):
-    rows = upper.shape[0] + lower.shape[0]
+def call_experts(units, routed, shared, model_width, expert_count):
+    rows = sum(u.shape[0] for u in units)
     column = model_width // 2
-    scratch = [pltpu.VMEM((rows, model_width), jnp.float32)]
-    if streamed:
-        scratch += [pltpu.SemaphoreType.DMA((len(streamed),))]
-        scratch += [pltpu.VMEM(w.shape, w.dtype) for w in streamed]
     return pl.pallas_call(
         functools.partial(
             expert_kernel,
-            held_count=len(held),
-            stream_count=len(streamed),
+            unit_count=len(units),
+            routed_count=len(routed),
+            shared_count=len(shared),
             expert_count=expert_count,
         ),
         out_shape=(
             jax.ShapeDtypeStruct((rows, column), jnp.float32),
             jax.ShapeDtypeStruct((rows, column), jnp.bfloat16),
         ),
-        in_specs=[VMEM] * (2 + len(held)) + [pl.BlockSpec(memory_space=pltpu.HBM)] * len(streamed),
-        out_specs=(VMEM, VMEM),
-        scratch_shapes=scratch,
+        in_specs=[VMEM] * (len(units) + len(routed) + len(shared)),
+        out_specs=(VMEM,) * 2,
+        scratch_shapes=[pltpu.VMEM((rows, model_width), jnp.float32)],
         compiler_params=within(16),
         name="experts",
-    )(upper, lower, *held, *[pltpu.with_memory_space_constraint(w, pltpu.HBM) for w in streamed])
+    )(*units, *routed, *shared)
 
 
 def column_order(head_count):
@@ -255,8 +285,8 @@
     return spread
 
 
-def far_order(far_count):
-    return [0] + [k for k in (2, 1) if k < far_count] + list(range(3, far_count))
+def groups_of(far_count):
+    return [[k] for k in range(far_count)]
 
 
 def per_device(
@@ -283,9 +313,6 @@
     tp_count = lax.axis_size("tp")
     ep_count = lax.axis_size("ep")
     far_count = ep_count // 2
-    own_tp = lax.axis_index("tp")
-    own_ep = lax.axis_index("ep")
-    core = own_tp % 2
     local_count = gate_weight.shape[0]
     expert_count = local_count * ep_count
 
@@ -298,8 +325,14 @@
         in_specs=[VMEM] * 4,
         out_specs=VMEM,
         scratch_shapes=[pltpu.VMEM((tok_rows, tail_width), jnp.float32)],
+        compiler_params=within(8),
         name="tokens",
-    )(second_rows, second_gain.reshape(1, -1), route_ids.T, route_weights.T)
+    )(
+        far_off(second_rows),
+        far_off(second_gain.reshape(1, -1)),
+        far_off(route_ids.T),
+        far_off(route_weights.T),
+    )
 
     far_units = [unit]
     for k in range(1, far_count):
@@ -307,32 +340,24 @@
     near_units = [swap(u, "ep", 1) for u in far_units]
 
     first_rows = query_latent.shape[0]
-    half_keys = first_rows // 2
+    latent_width = keyval_latent.shape[1]
     head_count = query_weight.shape[1] // (NOPE + ROPE)
     turned = head_count * ROPE
-    lane_pair = np.arange(turned) % (ROPE // 2)
-    inverse = 1.0 / ROPE_BASE ** (lane_pair.astype(np.float32) * 2.0 / ROPE)
-    positions = (own_ep * first_rows).astype(jnp.float32) + jnp.arange(
-        first_rows, dtype=jnp.float32
-    )
-    angles = positions[:, None] * jnp.asarray(inverse, jnp.float32)[None, :]
-    cosine = jnp.cos(angles)
-    sine = jnp.sin(angles)
-    latent_width = keyval_latent.shape[1]
+    inverse = far_off(jnp.asarray(inverses(turned)))
     key_unit = pl.pallas_call(
         key_kernel,
-        out_shape=jax.ShapeDtypeStruct((half_keys, latent_width + turned), jnp.bfloat16),
-        in_specs=[VMEM] * 6,
+        out_shape=jax.ShapeDtypeStruct((first_rows // 2, latent_width + turned), jnp.bfloat16),
+        in_specs=[VMEM] * 5,
         out_specs=VMEM,
-        scratch_shapes=[pltpu.VMEM((first_rows, 2 * turned), jnp.float32)],
+        scratch_shapes=[pltpu.VMEM((first_rows, turned), jnp.float32)],
+        compiler_params=within(8),
         name="keys",
     )(
-        keyval_latent,
-        keyval_gain.reshape(1, -1),
-        rotary_key.T,
-        cosine,
-        sine,
-        jnp.asarray(key_spread(head_count), jnp.bfloat16),
+        far_off(keyval_latent),
+        far_off(keyval_gain.reshape(1, -1)),
+        far_off(rotary_key.T),
+        far_off(jnp.asarray(key_spread(head_count), jnp.bfloat16)),
+        inverse,
     )
     far_keys = jnp.concatenate(
         [key_unit] + [swap(key_unit, "ep", 2 * k) for k in range(1, far_count)], 0
@@ -342,6 +367,17 @@
 
     own_shared = (shared_gate, shared_up, shared_down)
     own_routed = (gate_weight, up_weight, down_weight)
+    loads = own_routed + own_shared
+    held = pl.pallas_call(
+        hold_kernel,
+        out_shape=tuple(pltpu.VMEM(w.shape, w.dtype) for w in loads),
+        in_specs=[pl.BlockSpec(memory_space=pltpu.HBM)] * len(loads),
+        out_specs=(VMEM,) * len(loads),
+        scratch_shapes=[pltpu.SemaphoreType.DMA((len(loads),))],
+        compiler_params=within(8),
+        name="hold",
+    )(*[far_off(w) for w in loads])
+    near_routed, near_shared = tuple(held[:3]), tuple(held[3:])
     other_shared = tuple(swap(w, "tp", 1) for w in own_shared)
     other_routed = tuple(swap(w, "tp", 1) for w in own_routed)
 
@@ -350,45 +386,56 @@
         out_shape=jax.ShapeDtypeStruct(
             (first_rows, head_count * (NOPE + VDIM) + turned), jnp.bfloat16
         ),
-        in_specs=[VMEM] * 6,
+        in_specs=[VMEM] * 5,
         out_specs=VMEM,
         compiler_params=within(12),
         name="queries",
     )(
-        query_latent,
-        query_gain.reshape(1, -1),
-        query_weight,
-        jnp.asarray(column_order(head_count), jnp.bfloat16),
-        cosine,
-        sine,
-    )
-
-    arrived = None
-    for k in far_order(far_count):
+        far_off(query_latent),
+        far_off(query_gain.reshape(1, -1)),
+        far_off(query_weight),
+        far_off(jnp.asarray(column_order(head_count), jnp.bfloat16)),
+        inverse,
+    )
+
+    arrived = []
+    for group in groups_of(far_count):
         keep, send = call_experts(
-            far_units[k],
-            near_units[k],
-            other_routed + own_routed if k else other_routed,
-            () if k else own_shared + other_shared + own_routed,
+            [far_units[k] for k in group] + [near_units[k] for k in group],
+            other_routed + near_routed,
+            near_shared + other_shared if 0 in group else (),
             model_width,
             expert_count,
         )
         got = swap(send, "tp", 2)
-        lower = (keep[half_rows:] + got[half_rows:].astype(jnp.float32)).astype(jnp.bfloat16)
-        upper = keep[:half_rows] + got[:half_rows].astype(jnp.float32)
-        total = upper + swap(lower, "ep", 1).astype(jnp.float32)
-        if k:
-            total = swap(total.astype(jnp.bfloat16), "ep", 2 * k).astype(jnp.float32)
-        arrived = total if arrived is None else arrived + total
-    quarter_width = model_width // 4
-    mine = lax.dynamic_slice_in_dim(arrived, core * quarter_width, quarter_width, 1)
-    other = lax.dynamic_slice_in_dim(arrived, (1 - core) * quarter_width, quarter_width, 1)
-    mine = mine.astype(jnp.bfloat16)
-    other = swap(other.astype(jnp.bfloat16), "tp", 1)
-    first = core == 0
-    expert_mix = jnp.concatenate(
-        [jnp.where(first, mine, other), jnp.where(first, other, mine)], 0
-    )
+        rows = keep.shape[0] // 2
+        lower = (keep[rows:] + got[rows:].astype(jnp.float32)).astype(jnp.bfloat16)
+        back = swap(lower, "ep", 1)
+        for at, k in enumerate(group):
+            span = slice(at * half_rows, (at + 1) * half_rows)
+            total = keep[span] + got[span].astype(jnp.float32) + back[span].astype(jnp.float32)
+            if k:
+                total = swap(total.astype(jnp.bfloat16), "ep", 2 * k)
+            arrived.append(total)
+    mine_shape = jax.ShapeDtypeStruct((half_rows, model_width // 4), jnp.bfloat16)
+    mine, other = pl.pallas_call(
+        sum_kernel,
+        out_shape=(mine_shape, mine_shape),
+        in_specs=[VMEM] * len(arrived),
+        out_specs=(VMEM, VMEM),
+        scratch_shapes=[pltpu.VMEM((half_rows, model_width // 2), jnp.float32)],
+        compiler_params=within(4 + ep_count // 4),
+        name="sum_up",
+    )(*arrived)
+    other = swap(other, "tp", 1)
+    expert_mix = pl.pallas_call(
+        join_kernel,
+        out_shape=jax.ShapeDtypeStruct((tok_rows, model_width // 4), jnp.bfloat16),
+        in_specs=[VMEM, VMEM],
+        out_specs=VMEM,
+        compiler_params=within(4),
+        name="join",
+    )(mine, other)
 
     quarter = first_rows // tp_count
     keep, send = pl.pallas_call(

time: 132 us -> 100 us (0.76)
  local copies, waits for them, and re-layouts: 16.3 us -> 0.61 us
  waiting for transfers between devices: 57.9 us -> 44.4 us
  other arithmetic: 6.32 us -> 1.26 us
  starting transfers between devices: 33.8 us -> 36.7 us
    unnamed x74 -> x12, local copies, waits for them, and re-layouts: 15.6 us -> 0.03 us
    ppermute x33, waiting for transfers between devices: 57.9 us -> 44.4 us  [swap(): return lax.ppermute(values, axis, [(i, i ^ mask) for i in range(count)])]
    ppermute x33, starting transfers between devices: 33.8 us -> 36.7 us  [swap(): return lax.ppermute(values, axis, [(i, i ^ mask) for i in range(count)])]
    convert_element_type x7, other arithmetic: 2.06 us -> 0.24 us  [the longest x3 0.13 us: per_device(): total = swap(total.astype(jnp.bfloat16), 'ep', 2 * k)]
    pallas_call x1, Pallas kernels: 1.06 us -> 2.56 us  [per_device(): pl.pallas_call(query_kernel, out_shape=jax.ShapeDtypeStruct((first_rows,...]
    pallas_call x5 -> x8, Pallas kernels: 9.96 us -> 9.76 us  [the longest x4 5.36 us: call_experts(): pl.pallas_call(functools.partial(expert_kernel, unit_count=len(units), ro...]
  transfers between devices with their start and end apart: 33 -> 33, of which waited for: 9 -> 13; matrix products, arithmetic and copies ran while one was open for 4% -> 2% of each run, Pallas kernels for 11% -> 14%
where the time goes in v1:
time: 100 us
  waiting for transfers between devices  44.4 us (44%)
  starting transfers between devices  36.7 us (37%)
  Pallas kernels  16.4 us (16%)
  other arithmetic  1.26 us (1%)
    ppermute x33, waiting for transfers between devices, swap(): return lax.ppermute(values, axis, [(i, i ^ mask) for i in range(count)])  44.4 us
    ppermute x33, starting transfers between devices, swap(): return lax.ppermute(values, axis, [(i, i ^ mask) for i in range(count)])  36.7 us
    pallas_call x4, Pallas kernels, call_experts(): pl.pallas_call(functools.partial(expert_kernel, unit_count=len(units), ro...  5.36 us
    pallas_call x1, Pallas kernels, per_device(): pl.pallas_call(functools.partial(attention_kernel, head_count=head_count,...  2.72 us
    pallas_call x1, Pallas kernels, per_device(): pl.pallas_call(query_kernel, out_shape=jax.ShapeDtypeStruct((first_rows,...  2.56 us
    pallas_call x1, Pallas kernels, per_device(): pl.pallas_call(hold_kernel, out_shape=tuple((pltpu.VMEM(w.shape, w.dtype)...  2.35 us
  transfers between devices with their start and end apart: 33, of which 13 were waited for; matrix products, arithmetic and copies ran while one was open for 2% of the time, Pallas kernels for 14%

profile of v1, /device:TPU:0, one launch (start us, length us, event | category | flops | bytes accessed | tf_op | source)
XLA Modules:
  0.0 100.2 jit_solution(12085920690187971353)
XLA Ops:
  0.6 1.3 %tokens.1.refs_0_ = bf16[64,2176]{1,0:T(8,128)(2,1)S(1)} custom-call(bf16[128,2048]{1,0:T(8,128)(2,1)} %rows.1, f32[1,2048]{1,0:T(1,128)} %bitcast.5, s32[4,128]{1,0:T(4,128)} %bitcast.7, f32[4,128]{1,0:T(4,128)} %bitcast.8), custom_call_target="tpu_custom_call" | custom-call | tf_op jit(solution)/shard_map/tokens/pallas_call | solution.py:322
  2.0 3.1 %collective-permute-start.8 = (bf16[64,2176]{1,0:T(8,128)(2,1)S(1)}, bf16[64,2176]{1,0:T(8,128)(2,1)S(1)}, u32[]{:S(2)}, u32[]{:S(2)}) collective-permute-start(bf16[64,2176]{1,0:T(8,128)(2,1)S(1)} %tokens.1.refs_0_), channel_id=1, source_target_pairs={{0,4},{4,0},{8,12},{12,8},{16,20},{20,16},{24,28},{28,24},{1,5},{5... | collective-permute-start | bytes 835592 | tf_op jit(solution)/shard_map/ppermute | solution.py:41
  5.0 1.6 %collective-permute-start.17 = (bf16[64,2176]{1,0:T(8,128)(2,1)S(1)}, bf16[64,2176]{1,0:T(8,128)(2,1)S(1)}, u32[]{:S(2)}, u32[]{:S(2)}) collective-permute-start(bf16[64,2176]{1,0:T(8,128)(2,1)S(1)} %tokens.1.refs_0_), channel_id=1, source_target_pairs={{0,8},{4,12},{8,0},{12,4},{16,24},{20,28},{24,16},{28,20},{1,9},{5... | collective-permute-start | bytes 835592 | tf_op jit(solution)/shard_map/ppermute | solution.py:41
  6.6 1.3 %keys.1 = bf16[64,640]{1,0:T(8,128)(2,1)S(1)} custom-call(bf16[128,512]{1,0:T(8,128)(2,1)} %latent.3, f32[1,512]{1,0:T(1,128)} %bitcast.9, bf16[32,128]{1,0:T(8,128)(2,1)} %bitcast.6, bf16[32,256]{1,0:T(8,128)(2,1)} %constant.14.clone.spread, f32[1,128]{1,0:T(1,128)} %constant.13.clone.inverse), custom_call_target="tpu_custom_call" | custom-call | tf_op jit(solution)/shard_map/keys/pallas_call | solution.py:347
  7.9 2.5 %collective-permute-start.2 = (bf16[64,640]{1,0:T(8,128)(2,1)S(1)}, bf16[64,640]{1,0:T(8,128)(2,1)S(1)}, u32[]{:S(2)}, u32[]{:S(2)}) collective-permute-start(bf16[64,640]{1,0:T(8,128)(2,1)S(1)} %keys.1), channel_id=1, source_target_pairs={{0,24},{4,28},{8,16},{12,20},{16,8},{20,12},{24,0},{28,4},{1,25},{... | collective-permute-start | bytes 245768 | tf_op jit(solution)/shard_map/ppermute | solution.py:41
  10.7 1.7 %collective-permute-start = (bf16[64,640]{1,0:T(8,128)(2,1)S(1)}, bf16[64,640]{1,0:T(8,128)(2,1)S(1)}, u32[]{:S(2)}, u32[]{:S(2)}) collective-permute-start(bf16[64,640]{1,0:T(8,128)(2,1)S(1)} %keys.1), channel_id=1, source_target_pairs={{0,8},{4,12},{8,0},{12,4},{16,24},{20,28},{24,16},{28,20},{1,9},{5... | collective-permute-start | bytes 245768 | tf_op jit(solution)/shard_map/ppermute | solution.py:41
  12.4 6.0 %collective-permute-done.2 = bf16[64,640]{1,0:T(8,128)(2,1)S(1)} collective-permute-done((bf16[64,640]{1,0:T(8,128)(2,1)S(1)}, bf16[64,640]{1,0:T(8,128)(2,1)S(1)}, u32[]{:S(2)}, u32[]{:S(2)}) %collective-permute-start.2) | collective-permute-done | bytes 81952 | tf_op jit(solution)/shard_map/ppermute | solution.py:41
  19.5 3.9 %collective-permute-start.27 = (bf16[64,2176]{1,0:T(8,128)(2,1)S(1)}, bf16[64,2176]{1,0:T(8,128)(2,1)S(1)}, u32[]{:S(2)}, u32[]{:S(2)}) collective-permute-start(bf16[64,2176]{1,0:T(8,128)(2,1)S(1)} %tokens.1.refs_0_), channel_id=1, source_target_pairs={{0,24},{4,28},{8,16},{12,20},{16,8},{20,12},{24,0},{28,4},{1,25},{... | collective-permute-start | bytes 835592 | tf_op jit(solution)/shard_map/ppermute | solution.py:41
  23.9 14.4 %collective-permute-done.22.refs_0_ = bf16[64,2176]{1,0:T(8,128)(2,1)S(1)} collective-permute-done((bf16[64,2176]{1,0:T(8,128)(2,1)S(1)}, bf16[64,2176]{1,0:T(8,128)(2,1)S(1)}, u32[]{:S(2)}, u32[]{:S(2)}) %collective-permute-start.22) | collective-permute-done | bytes 278560 | tf_op jit(solution)/shard_map/ppermute | solution.py:41
  38.9 1.0 %collective-permute-done.4.refs_2_ = bf16[256,640]{1,0:T(8,128)(2,1)S(1)} collective-permute-done((bf16[256,640]{1,0:T(8,128)(2,1)S(1)}, bf16[256,640]{1,0:T(8,128)(2,1)S(1)}, u32[]{:S(2)}, u32[]{:S(2)}) %collective-permute-start.4) | collective-permute-done | bytes 327712 | tf_op jit(solution)/shard_map/ppermute | solution.py:41
  42.0 2.6 %queries.1 = bf16[128,640]{1,0:T(8,128)(2,1)S(1)} custom-call(bf16[128,768]{1,0:T(8,128)(2,1)} %latent.2, f32[1,768]{1,0:T(1,128)} %reshape.22.gain, bf16[768,384]{1,0:T(8,128)(2,1)} %weight.1, bf16[384,768]{1,0:T(8,128)(2,1)} %constant.15.clone.order, f32[1,128]{1,0:T(1,128)} %constant.13.clone.inverse), custom_call_target="tpu_custom_call" | custom-call | tf_op jit(solution)/shard_map/queries/pallas_call | solution.py:384
  44.6 2.7 %attention.1 = (f32[64,2048]{1,0:T(8,128)S(1)}, bf16[64,2048]{1,0:T(8,128)(2,1)S(1)}) custom-call(bf16[128,640]{1,0:T(8,128)(2,1)S(1)} %queries.1, bf16[256,640]{1,0:T(8,128)(2,1)S(1)} %pad_maximum_fusion.refs_0_, bf16[256,640]{1,0:T(8,128)(2,1)S(1)} %collective-permute-done.3.refs_1_, bf16[256,640]{1,0:T(8,128)(2,1)S(1)} %collective-permute-done.4.refs_2_, ...), custom_call_target="tpu_custom_call" | custom-call | tf_op jit(solution)/shard_map/attention/pallas_call | solution.py:441
  49.7 1.3 %collective-permute-start.28 = (bf16[64,2176]{1,0:T(8,128)(2,1)S(1)}, bf16[64,2176]{1,0:T(8,128)(2,1)S(1)}, u32[]{:S(2)}, u32[]{:S(2)}) collective-permute-start(bf16[64,2176]{1,0:T(8,128)(2,1)S(1)} %collective-permute-done.27.refs_0_), channel_id=1, source_target_pairs={{0,4},{4,0},{8,12},{12,8},{16,20},{20,16},{24,28},{28,24},{1,5},{5... | collective-permute-start | bytes 835592 | tf_op jit(solution)/shard_map/ppermute | solution.py:41
  51.0 1.6 %collective-permute-start.7 = (bf16[32,2048]{1,0:T(8,128)(2,1)S(1)}, bf16[32,2048]{1,0:T(8,128)(2,1)S(1)}, u32[]{:S(2)}, u32[]{:S(2)}) collective-permute-start(bf16[32,2048]{1,0:T(8,128)(2,1)S(1)} %add_convert_fusion.7), channel_id=1, source_target_pairs={{0,2},{1,3},{2,0},{3,1},{4,6},{5,7},{6,4},{7,5},{8,10},{9,11},{10,... | collective-permute-start | bytes 393224 | tf_op jit(solution)/shard_map/ppermute | solution.py:41
  52.6 2.4 %hold.1 = (bf16[1,2048,256]{2,1,0:T(8,128)(2,1)S(1)}, bf16[1,2048,256]{2,1,0:T(8,128)(2,1)S(1)}, bf16[1,256,2048]{2,1,0:T(8,128)(2,1)S(1)}, bf16[2048,128]{1,0:T...) custom-call(bf16[1,2048,256]{2,1,0:T(8,128)(2,1)} %refs_0_.1, ...), custom_call_target="tpu_custom_call" | custom-call | tf_op jit(solution)/shard_map/hold/pallas_call | solution.py:371
  55.0 1.8 %experts.4 = (f32[128,1024]{1,0:T(8,128)S(1)}, bf16[128,1024]{1,0:T(8,128)(2,1)S(1)}) custom-call(bf16[64,2176]{1,0:T(8,128)(2,1)S(1)} %tokens.1.refs_0_, bf16[64,2176]{1,0:T(8,128)(2,1)S(1)} %collective-permute-done.8.refs_1_, bf16[1,2048,256]{2,1,0:T(8,128)(2,1)S(1)} %collective-permute-done.9.refs_2_, ...), custom_call_target="tpu_custom_call" | custom-call | tf_op jit(solution)/shard_map/experts/pallas_call | solution.py:234
  57.4 1.2 %experts.5 = (f32[128,1024]{1,0:T(8,128)S(1)}, bf16[128,1024]{1,0:T(8,128)(2,1)S(1)}) custom-call(bf16[64,2176]{1,0:T(8,128)(2,1)S(1)} %collective-permute-done.17.refs_0_, bf16[64,2176]{1,0:T(8,128)(2,1)S(1)} %collective-permute-done.18.refs_1_, bf16[1,2048,256]{2,1,0:T(8,128)(2,1)S(1)} %collective-permute-done.9.refs_2_, ...), custom_call_target="tpu_custom_call" | custom-call | tf_op jit(solution)/shard_map/experts/pallas_call | solution.py:234
  58.6 1.6 %collective-permute-start.19 = (bf16[128,1024]{1,0:T(8,128)(2,1)S(1)}, bf16[128,1024]{1,0:T(8,128)(2,1)S(1)}, u32[]{:S(2)}, u32[]{:S(2)}) collective-permute-start(bf16[128,1024]{1,0:T(8,128)(2,1)S(1)} %get-tuple-element.31), channel_id=1, source_target_pairs={{0,2},{1,3},{2,0},{3,1},{4,6},{5,7},{6,4},{7,5},{8,10},{9,11},{10,... | collective-permute-start | bytes 786440 | tf_op jit(solution)/shard_map/ppermute | solution.py:41
  60.1 3.1 %collective-permute-done.23.refs_1_ = bf16[64,2176]{1,0:T(8,128)(2,1)S(1)} collective-permute-done((bf16[64,2176]{1,0:T(8,128)(2,1)S(1)}, bf16[64,2176]{1,0:T(8,128)(2,1)S(1)}, u32[]{:S(2)}, u32[]{:S(2)}) %collective-permute-start.23) | collective-permute-done | bytes 278560 | tf_op jit(solution)/shard_map/ppermute | solution.py:41
  63.2 1.2 %experts.6 = (f32[128,1024]{1,0:T(8,128)S(1)}, bf16[128,1024]{1,0:T(8,128)(2,1)S(1)}) custom-call(bf16[64,2176]{1,0:T(8,128)(2,1)S(1)} %collective-permute-done.22.refs_0_, bf16[64,2176]{1,0:T(8,128)(2,1)S(1)} %collective-permute-done.23.refs_1_, bf16[1,2048,256]{2,1,0:T(8,128)(2,1)S(1)} %collective-permute-done.9.refs_2_, ...), custom_call_target="tpu_custom_call" | custom-call | tf_op jit(solution)/shard_map/experts/pallas_call | solution.py:234
  64.4 1.6 %collective-permute-start.24 = (bf16[128,1024]{1,0:T(8,128)(2,1)S(1)}, bf16[128,1024]{1,0:T(8,128)(2,1)S(1)}, u32[]{:S(2)}, u32[]{:S(2)}) collective-permute-start(bf16[128,1024]{1,0:T(8,128)(2,1)S(1)} %get-tuple-element.33), channel_id=1, source_target_pairs={{0,2},{1,3},{2,0},{3,1},{4,6},{5,7},{6,4},{7,5},{8,10},{9,11},{10,... | collective-permute-start | bytes 786440 | tf_op jit(solution)/shard_map/ppermute | solution.py:41
  66.0 2.5 %collective-permute-done.28.refs_1_ = bf16[64,2176]{1,0:T(8,128)(2,1)S(1)} collective-permute-done((bf16[64,2176]{1,0:T(8,128)(2,1)S(1)}, bf16[64,2176]{1,0:T(8,128)(2,1)S(1)}, u32[]{:S(2)}, u32[]{:S(2)}) %collective-permute-start.28) | collective-permute-done | bytes 278560 | tf_op jit(solution)/shard_map/ppermute | solution.py:41
  68.5 1.2 %experts.7 = (f32[128,1024]{1,0:T(8,128)S(1)}, bf16[128,1024]{1,0:T(8,128)(2,1)S(1)}) custom-call(bf16[64,2176]{1,0:T(8,128)(2,1)S(1)} %collective-permute-done.27.refs_0_, bf16[64,2176]{1,0:T(8,128)(2,1)S(1)} %collective-permute-done.28.refs_1_, bf16[1,2048,256]{2,1,0:T(8,128)(2,1)S(1)} %collective-permute-done.9.refs_2_, ...), custom_call_target="tpu_custom_call" | custom-call | tf_op jit(solution)/shard_map/experts/pallas_call | solution.py:234
  69.7 1.6 %collective-permute-start.29 = (bf16[128,1024]{1,0:T(8,128)(2,1)S(1)}, bf16[128,1024]{1,0:T(8,128)(2,1)S(1)}, u32[]{:S(2)}, u32[]{:S(2)}) collective-permute-start(bf16[128,1024]{1,0:T(8,128)(2,1)S(1)} %get-tuple-element.35), channel_id=1, source_target_pairs={{0,2},{1,3},{2,0},{3,1},{4,6},{5,7},{6,4},{7,5},{8,10},{9,11},{10,... | collective-permute-start | bytes 786440 | tf_op jit(solution)/shard_map/ppermute | solution.py:41
  72.0 1.6 %collective-permute-start.20 = (bf16[64,1024]{1,0:T(8,128)(2,1)S(1)}, bf16[64,1024]{1,0:T(8,128)(2,1)S(1)}, u32[]{:S(2)}, u32[]{:S(2)}) collective-permute-start(bf16[64,1024]{1,0:T(8,128)(2,1)S(1)} %add_convert_fusion.5), channel_id=1, source_target_pairs={{0,4},{4,0},{8,12},{12,8},{16,20},{20,16},{24,28},{28,24},{1,5},{5... | collective-permute-start | bytes 393224 | tf_op jit(solution)/shard_map/ppermute | solution.py:41
  73.6 3.6 %collective-permute-done.24 = bf16[128,1024]{1,0:T(8,128)(2,1)S(1)} collective-permute-done((bf16[128,1024]{1,0:T(8,128)(2,1)S(1)}, bf16[128,1024]{1,0:T(8,128)(2,1)S(1)}, u32[]{:S(2)}, u32[]{:S(2)}) %collective-permute-start.24) | collective-permute-done | bytes 262176 | tf_op jit(solution)/shard_map/ppermute | solution.py:41
  77.3 0.8 collective-permute-start.25
  78.1 3.2 %collective-permute-done.29 = bf16[128,1024]{1,0:T(8,128)(2,1)S(1)} collective-permute-done((bf16[128,1024]{1,0:T(8,128)(2,1)S(1)}, bf16[128,1024]{1,0:T(8,128)(2,1)S(1)}, u32[]{:S(2)}, u32[]{:S(2)}) %collective-permute-start.29) | collective-permute-done | bytes 262176 | tf_op jit(solution)/shard_map/ppermute | solution.py:41
  82.0 5.4 %collective-permute-start.21 = (bf16[64,1024]{1,0:T(8,128)(2,1)S(1)}, bf16[64,1024]{1,0:T(8,128)(2,1)S(1)}, u32[]{:S(2)}, u32[]{:S(2)}) collective-permute-start(bf16[64,1024]{1,0:T(8,128)(2,1)S(1)} %add_convert_fusion.4), channel_id=1, source_target_pairs={{0,8},{4,12},{8,0},{12,4},{16,24},{20,28},{24,16},{28,20},{1,9},{5... | collective-permute-start | bytes 393224 | tf_op jit(solution)/shard_map/ppermute | solution.py:41
  87.6 2.5 %collective-permute-start.31 = (bf16[64,1024]{1,0:T(8,128)(2,1)S(1)}, bf16[64,1024]{1,0:T(8,128)(2,1)S(1)}, u32[]{:S(2)}, u32[]{:S(2)}) collective-permute-start(bf16[64,1024]{1,0:T(8,128)(2,1)S(1)} %add_convert_fusion), channel_id=1, source_target_pairs={{0,24},{4,28},{8,16},{12,20},{16,8},{20,12},{24,0},{28,4},{1,25},{... | collective-permute-start | bytes 393224 | tf_op jit(solution)/shard_map/ppermute | solution.py:41
  90.2 1.1 %collective-permute-done.21.refs_0_ = bf16[64,1024]{1,0:T(8,128)(2,1)S(1)} collective-permute-done((bf16[64,1024]{1,0:T(8,128)(2,1)S(1)}, bf16[64,1024]{1,0:T(8,128)(2,1)S(1)}, u32[]{:S(2)}, u32[]{:S(2)}) %collective-permute-start.21) | collective-permute-done | bytes 131104 | tf_op jit(solution)/shard_map/ppermute | solution.py:41
  91.2 6.9 %collective-permute-done.26.refs_1_ = bf16[64,1024]{1,0:T(8,128)(2,1)S(1)} collective-permute-done((bf16[64,1024]{1,0:T(8,128)(2,1)S(1)}, bf16[64,1024]{1,0:T(8,128)(2,1)S(1)}, u32[]{:S(2)}, u32[]{:S(2)}) %collective-permute-start.26) | collective-permute-done | bytes 131104 | tf_op jit(solution)/shard_map/ppermute | solution.py:41
  (71 shorter events, 11.3 us)
Async XLA Ops:
  2.0 21.4 %collective-permute-start.8 = (bf16[64,2176]{1,0:T(8,128)(2,1)S(1)}, bf16[64,2176]{1,0:T(8,128)(2,1)S(1)}, u32[]{:S(2)}, u32[]{:S(2)}) collective-permute-start(bf16[64,2176]{1,0:T(8,128)(2,1)S(1)} %tokens.1.refs_0_), channel_id=1, source_target_pairs={{0,4},{4,0},{8,12},{12,8},{16,20},{20,16},{24,28},{28,24},{1,5},{5... | collective-permute-start | bytes 835592 | tf_op jit(solution)/shard_map/ppermute | solution.py:41
  5.0 18.4 %collective-permute-start.17 = (bf16[64,2176]{1,0:T(8,128)(2,1)S(1)}, bf16[64,2176]{1,0:T(8,128)(2,1)S(1)}, u32[]{:S(2)}, u32[]{:S(2)}) collective-permute-start(bf16[64,2176]{1,0:T(8,128)(2,1)S(1)} %tokens.1.refs_0_), channel_id=1, source_target_pairs={{0,8},{4,12},{8,0},{12,4},{16,24},{20,28},{24,16},{28,20},{1,9},{5... | collective-permute-start | bytes 835592 | tf_op jit(solution)/shard_map/ppermute | solution.py:41
  7.9 10.4 %collective-permute-start.2 = (bf16[64,640]{1,0:T(8,128)(2,1)S(1)}, bf16[64,640]{1,0:T(8,128)(2,1)S(1)}, u32[]{:S(2)}, u32[]{:S(2)}) collective-permute-start(bf16[64,640]{1,0:T(8,128)(2,1)S(1)} %keys.1), channel_id=1, source_target_pairs={{0,24},{4,28},{8,16},{12,20},{16,8},{20,12},{24,0},{28,4},{1,25},{... | collective-permute-start | bytes 245768 | tf_op jit(solution)/shard_map/ppermute | solution.py:41
  10.5 7.9 %collective-permute-start.1 = (bf16[64,640]{1,0:T(8,128)(2,1)S(1)}, bf16[64,640]{1,0:T(8,128)(2,1)S(1)}, u32[]{:S(2)}, u32[]{:S(2)}) collective-permute-start(bf16[64,640]{1,0:T(8,128)(2,1)S(1)} %keys.1), channel_id=1, source_target_pairs={{0,16},{4,20},{8,24},{12,28},{16,0},{20,4},{24,8},{28,12},{1,17},{... | collective-permute-start | bytes 245768 | tf_op jit(solution)/shard_map/ppermute | solution.py:41
  10.7 8.3 %collective-permute-start = (bf16[64,640]{1,0:T(8,128)(2,1)S(1)}, bf16[64,640]{1,0:T(8,128)(2,1)S(1)}, u32[]{:S(2)}, u32[]{:S(2)}) collective-permute-start(bf16[64,640]{1,0:T(8,128)(2,1)S(1)} %keys.1), channel_id=1, source_target_pairs={{0,8},{4,12},{8,0},{12,4},{16,24},{20,28},{24,16},{28,20},{1,9},{5... | collective-permute-start | bytes 245768 | tf_op jit(solution)/shard_map/ppermute | solution.py:41
  18.4 20.0 %collective-permute-start.22 = (bf16[64,2176]{1,0:T(8,128)(2,1)S(1)}, bf16[64,2176]{1,0:T(8,128)(2,1)S(1)}, u32[]{:S(2)}, u32[]{:S(2)}) collective-permute-start(bf16[64,2176]{1,0:T(8,128)(2,1)S(1)} %tokens.1.refs_0_), channel_id=1, source_target_pairs={{0,16},{4,20},{8,24},{12,28},{16,0},{20,4},{24,8},{28,12},{1,17},{... | collective-permute-start | bytes 835592 | tf_op jit(solution)/shard_map/ppermute | solution.py:41
  19.0 19.9 %collective-permute-start.3 = (bf16[256,640]{1,0:T(8,128)(2,1)S(1)}, bf16[256,640]{1,0:T(8,128)(2,1)S(1)}, u32[]{:S(2)}, u32[]{:S(2)}) collective-permute-start(bf16[256,640]{1,0:T(8,128)(2,1)S(1)} %pad_maximum_fusion.refs_0_), channel_id=1, source_target_pairs={{0,4},{4,0},{8,12},{12,8},{16,20},{20,16},{24,28},{28,24},{1,5},{5... | collective-permute-start | bytes 983048 | tf_op jit(solution)/shard_map/ppermute | solution.py:41
  19.5 18.8 %collective-permute-start.27 = (bf16[64,2176]{1,0:T(8,128)(2,1)S(1)}, bf16[64,2176]{1,0:T(8,128)(2,1)S(1)}, u32[]{:S(2)}, u32[]{:S(2)}) collective-permute-start(bf16[64,2176]{1,0:T(8,128)(2,1)S(1)} %tokens.1.refs_0_), channel_id=1, source_target_pairs={{0,24},{4,28},{8,16},{12,20},{16,8},{20,12},{24,0},{28,4},{1,25},{... | collective-permute-start | bytes 835592 | tf_op jit(solution)/shard_map/ppermute | solution.py:41
  23.4 16.7 %collective-permute-start.12 = (bf16[2048,128]{1,0:T(8,128)(2,1)S(1)}, bf16[2048,128]{1,0:T(8,128)(2,1)S(1)}, u32[]{:S(2)}, u32[]{:S(2)}) collective-permute-start(bf16[2048,128]{1,0:T(8,128)(2,1)S(1)} %copy-done.3), channel_id=1, source_target_pairs={{0,1},{1,0},{2,3},{3,2},{4,5},{5,4},{6,7},{7,6},{8,9},{9,8},{10,11... | collective-permute-start | bytes 1572872 | tf_op jit(solution)/shard_map/ppermute | solution.py:41
  23.4 26.3 %collective-permute-start.9 = (bf16[1,2048,256]{2,1,0:T(8,128)(2,1)S(1)}, bf16[1,2048,256]{2,1,0:T(8,128)(2,1)S(1)}, u32[]{:S(2)}, u32[]{:S(2)}) collective-permute-start(bf16[1,2048,256]{2,1,0:T(8,128)(2,1)S(1)} %copy-done.2), channel_id=1, source_target_pairs={{0,1},{1,0},{2,3},{3,2},{4,5},{5,4},{6,7},{7,6},{8,9},{9,8},{10,11... | collective-permute-start | bytes 3145736 | tf_op jit(solution)/shard_map/ppermute | solution.py:41
  38.4 1.6 %collective-permute-start.4 = (bf16[256,640]{1,0:T(8,128)(2,1)S(1)}, bf16[256,640]{1,0:T(8,128)(2,1)S(1)}, u32[]{:S(2)}, u32[]{:S(2)}) collective-permute-start(bf16[256,640]{1,0:T(8,128)(2,1)S(1)} %pad_maximum_fusion.refs_0_), channel_id=1, source_target_pairs={{0,1},{1,0},{2,3},{3,2},{4,5},{5,4},{6,7},{7,6},{8,9},{9,8},{10,11... | collective-permute-start | bytes 983048 | tf_op jit(solution)/shard_map/ppermute | solution.py:41
  38.4 9.0 %collective-permute-start.13 = (bf16[2048,128]{1,0:T(8,128)(2,1)}, bf16[2048,128]{1,0:T(8,128)(2,1)S(1)}, u32[]{:S(2)}, u32[]{:S(2)}) collective-permute-start(bf16[2048,128]{1,0:T(8,128)(2,1)} %refs_4_.3), channel_id=1, source_target_pairs={{0,1},{1,0},{2,3},{3,2},{4,5},{5,4},{6,7},{7,6},{8,9},{9,8},{10,11... | collective-permute-start | bytes 1572872 | tf_op jit(solution)/shard_map/ppermute | solution.py:41
  38.9 2.3 %collective-permute-start.5 = (bf16[256,640]{1,0:T(8,128)(2,1)S(1)}, bf16[256,640]{1,0:T(8,128)(2,1)S(1)}, u32[]{:S(2)}, u32[]{:S(2)}) collective-permute-start(bf16[256,640]{1,0:T(8,128)(2,1)S(1)} %collective-permute-done.3.refs_1_), channel_id=1, source_target_pairs={{0,1},{1,0},{2,3},{3,2},{4,5},{5,4},{6,7},{7,6},{8,9},{9,8},{10,11... | collective-permute-start | bytes 983048 | tf_op jit(solution)/shard_map/ppermute | solution.py:41
  40.0 11.1 %collective-permute-start.10 = (bf16[1,2048,256]{2,1,0:T(8,128)(2,1)}, bf16[1,2048,256]{2,1,0:T(8,128)(2,1)S(1)}, u32[]{:S(2)}, u32[]{:S(2)}) collective-permute-start(bf16[1,2048,256]{2,1,0:T(8,128)(2,1)} %refs_1_.1), channel_id=1, source_target_pairs={{0,1},{1,0},{2,3},{3,2},{4,5},{5,4},{6,7},{7,6},{8,9},{9,8},{10,11... | collective-permute-start | bytes 3145736 | tf_op jit(solution)/shard_map/ppermute | solution.py:41
  40.1 7.6 %collective-permute-start.14 = (bf16[128,2048]{1,0:T(8,128)(2,1)}, bf16[128,2048]{1,0:T(8,128)(2,1)S(1)}, u32[]{:S(2)}, u32[]{:S(2)}) collective-permute-start(bf16[128,2048]{1,0:T(8,128)(2,1)} %refs_5_.3), channel_id=1, source_target_pairs={{0,1},{1,0},{2,3},{3,2},{4,5},{5,4},{6,7},{7,6},{8,9},{9,8},{10,11... | collective-permute-start | bytes 1572872 | tf_op jit(solution)/shard_map/ppermute | solution.py:41
  41.2 13.8 %collective-permute-start.11 = (bf16[1,256,2048]{2,1,0:T(8,128)(2,1)}, bf16[1,256,2048]{2,1,0:T(8,128)(2,1)S(1)}, u32[]{:S(2)}, u32[]{:S(2)}) collective-permute-start(bf16[1,256,2048]{2,1,0:T(8,128)(2,1)} %refs_2_.1), channel_id=1, source_target_pairs={{0,1},{1,0},{2,3},{3,2},{4,5},{5,4},{6,7},{7,6},{8,9},{9,8},{10,11... | collective-permute-start | bytes 3145736 | tf_op jit(solution)/shard_map/ppermute | solution.py:41
  47.4 1.6 %collective-permute-start.6 = (bf16[64,2048]{1,0:T(8,128)(2,1)S(1)}, bf16[64,2048]{1,0:T(8,128)(2,1)S(1)}, u32[]{:S(2)}, u32[]{:S(2)}) collective-permute-start(bf16[64,2048]{1,0:T(8,128)(2,1)S(1)} %get-tuple-element.21), channel_id=1, source_target_pairs={{0,1},{1,0},{2,3},{3,2},{4,5},{5,4},{6,7},{7,6},{8,9},{9,8},{10,11... | collective-permute-start | bytes 786440 | tf_op jit(solution)/shard_map/ppermute | solution.py:41
  47.7 9.7 %collective-permute-start.18 = (bf16[64,2176]{1,0:T(8,128)(2,1)S(1)}, bf16[64,2176]{1,0:T(8,128)(2,1)S(1)}, u32[]{:S(2)}, u32[]{:S(2)}) collective-permute-start(bf16[64,2176]{1,0:T(8,128)(2,1)S(1)} %collective-permute-done.17.refs_0_), channel_id=1, source_target_pairs={{0,4},{4,0},{8,12},{12,8},{16,20},{20,16},{24,28},{28,24},{1,5},{5... | collective-permute-start | bytes 835592 | tf_op jit(solution)/shard_map/ppermute | solution.py:41
  49.0 14.2 %collective-permute-start.23 = (bf16[64,2176]{1,0:T(8,128)(2,1)S(1)}, bf16[64,2176]{1,0:T(8,128)(2,1)S(1)}, u32[]{:S(2)}, u32[]{:S(2)}) collective-permute-start(bf16[64,2176]{1,0:T(8,128)(2,1)S(1)} %collective-permute-done.22.refs_0_), channel_id=1, source_target_pairs={{0,4},{4,0},{8,12},{12,8},{16,20},{20,16},{24,28},{28,24},{1,5},{5... | collective-permute-start | bytes 835592 | tf_op jit(solution)/shard_map/ppermute | solution.py:41
  49.7 18.7 %collective-permute-start.28 = (bf16[64,2176]{1,0:T(8,128)(2,1)S(1)}, bf16[64,2176]{1,0:T(8,128)(2,1)S(1)}, u32[]{:S(2)}, u32[]{:S(2)}) collective-permute-start(bf16[64,2176]{1,0:T(8,128)(2,1)S(1)} %collective-permute-done.27.refs_0_), channel_id=1, source_target_pairs={{0,4},{4,0},{8,12},{12,8},{16,20},{20,16},{24,28},{28,24},{1,5},{5... | collective-permute-start | bytes 835592 | tf_op jit(solution)/shard_map/ppermute | solution.py:41
  51.0 20.2 %collective-permute-start.7 = (bf16[32,2048]{1,0:T(8,128)(2,1)S(1)}, bf16[32,2048]{1,0:T(8,128)(2,1)S(1)}, u32[]{:S(2)}, u32[]{:S(2)}) collective-permute-start(bf16[32,2048]{1,0:T(8,128)(2,1)S(1)} %add_convert_fusion.7), channel_id=1, source_target_pairs={{0,2},{1,3},{2,0},{3,1},{4,6},{5,7},{6,4},{7,5},{8,10},{9,11},{10,... | collective-permute-start | bytes 393224 | tf_op jit(solution)/shard_map/ppermute | solution.py:41
  56.8 14.6 %collective-permute-start.15 = (bf16[128,1024]{1,0:T(8,128)(2,1)S(1)}, bf16[128,1024]{1,0:T(8,128)(2,1)S(1)}, u32[]{:S(2)}, u32[]{:S(2)}) collective-permute-start(bf16[128,1024]{1,0:T(8,128)(2,1)S(1)} %get-tuple-element.29), channel_id=1, source_target_pairs={{0,2},{1,3},{2,0},{3,1},{4,6},{5,7},{6,4},{7,5},{8,10},{9,11},{10,... | collective-permute-start | bytes 786440 | tf_op jit(solution)/shard_map/ppermute | solution.py:41
  58.6 13.4 %collective-permute-start.19 = (bf16[128,1024]{1,0:T(8,128)(2,1)S(1)}, bf16[128,1024]{1,0:T(8,128)(2,1)S(1)}, u32[]{:S(2)}, u32[]{:S(2)}) collective-permute-start(bf16[128,1024]{1,0:T(8,128)(2,1)S(1)} %get-tuple-element.31), channel_id=1, source_target_pairs={{0,2},{1,3},{2,0},{3,1},{4,6},{5,7},{6,4},{7,5},{8,10},{9,11},{10,... | collective-permute-start | bytes 786440 | tf_op jit(solution)/shard_map/ppermute | solution.py:41
  64.4 12.9 %collective-permute-start.24 = (bf16[128,1024]{1,0:T(8,128)(2,1)S(1)}, bf16[128,1024]{1,0:T(8,128)(2,1)S(1)}, u32[]{:S(2)}, u32[]{:S(2)}) collective-permute-start(bf16[128,1024]{1,0:T(8,128)(2,1)S(1)} %get-tuple-element.33), channel_id=1, source_target_pairs={{0,2},{1,3},{2,0},{3,1},{4,6},{5,7},{6,4},{7,5},{8,10},{9,11},{10,... | collective-permute-start | bytes 786440 | tf_op jit(solution)/shard_map/ppermute | solution.py:41
  69.7 11.7 %collective-permute-start.29 = (bf16[128,1024]{1,0:T(8,128)(2,1)S(1)}, bf16[128,1024]{1,0:T(8,128)(2,1)S(1)}, u32[]{:S(2)}, u32[]{:S(2)}) collective-permute-start(bf16[128,1024]{1,0:T(8,128)(2,1)S(1)} %get-tuple-element.35), channel_id=1, source_target_pairs={{0,2},{1,3},{2,0},{3,1},{4,6},{5,7},{6,4},{7,5},{8,10},{9,11},{10,... | collective-permute-start | bytes 786440 | tf_op jit(solution)/shard_map/ppermute | solution.py:41
  71.4 18.7 %collective-permute-start.16 = (bf16[64,1024]{1,0:T(8,128)(2,1)S(1)}, bf16[64,1024]{1,0:T(8,128)(2,1)S(1)}, u32[]{:S(2)}, u32[]{:S(2)}) collective-permute-start(bf16[64,1024]{1,0:T(8,128)(2,1)S(1)} %add_convert_fusion.6), channel_id=1, source_target_pairs={{0,4},{4,0},{8,12},{12,8},{16,20},{20,16},{24,28},{28,24},{1,5},{5... | collective-permute-start | bytes 393224 | tf_op jit(solution)/shard_map/ppermute | solution.py:41
  72.0 9.9 %collective-permute-start.20 = (bf16[64,1024]{1,0:T(8,128)(2,1)S(1)}, bf16[64,1024]{1,0:T(8,128)(2,1)S(1)}, u32[]{:S(2)}, u32[]{:S(2)}) collective-permute-start(bf16[64,1024]{1,0:T(8,128)(2,1)S(1)} %add_convert_fusion.5), channel_id=1, source_target_pairs={{0,4},{4,0},{8,12},{12,8},{16,20},{20,16},{24,28},{28,24},{1,5},{5... | collective-permute-start | bytes 393224 | tf_op jit(solution)/shard_map/ppermute | solution.py:41
  77.3 10.1 %collective-permute-start.25 = (bf16[64,1024]{1,0:T(8,128)(2,1)S(1)}, bf16[64,1024]{1,0:T(8,128)(2,1)S(1)}, u32[]{:S(2)}, u32[]{:S(2)}) collective-permute-start(bf16[64,1024]{1,0:T(8,128)(2,1)S(1)} %add_convert_fusion.3), channel_id=1, source_target_pairs={{0,4},{4,0},{8,12},{12,8},{16,20},{20,16},{24,28},{28,24},{1,5},{5... | collective-permute-start | bytes 393224 | tf_op jit(solution)/shard_map/ppermute | solution.py:41
  81.3 6.2 %collective-permute-start.30 = (bf16[64,1024]{1,0:T(8,128)(2,1)S(1)}, bf16[64,1024]{1,0:T(8,128)(2,1)S(1)}, u32[]{:S(2)}, u32[]{:S(2)}) collective-permute-start(bf16[64,1024]{1,0:T(8,128)(2,1)S(1)} %add_convert_fusion.1), channel_id=1, source_target_pairs={{0,4},{4,0},{8,12},{12,8},{16,20},{20,16},{24,28},{28,24},{1,5},{5... | collective-permute-start | bytes 393224 | tf_op jit(solution)/shard_map/ppermute | solution.py:41
  82.0 9.3 %collective-permute-start.21 = (bf16[64,1024]{1,0:T(8,128)(2,1)S(1)}, bf16[64,1024]{1,0:T(8,128)(2,1)S(1)}, u32[]{:S(2)}, u32[]{:S(2)}) collective-permute-start(bf16[64,1024]{1,0:T(8,128)(2,1)S(1)} %add_convert_fusion.4), channel_id=1, source_target_pairs={{0,8},{4,12},{8,0},{12,4},{16,24},{20,28},{24,16},{28,20},{1,9},{5... | collective-permute-start | bytes 393224 | tf_op jit(solution)/shard_map/ppermute | solution.py:41
  87.4 10.7 %collective-permute-start.26 = (bf16[64,1024]{1,0:T(8,128)(2,1)S(1)}, bf16[64,1024]{1,0:T(8,128)(2,1)S(1)}, u32[]{:S(2)}, u32[]{:S(2)}) collective-permute-start(bf16[64,1024]{1,0:T(8,128)(2,1)S(1)} %add_convert_fusion.2), channel_id=1, source_target_pairs={{0,16},{4,20},{8,24},{12,28},{16,0},{20,4},{24,8},{28,12},{1,17},{... | collective-permute-start | bytes 393224 | tf_op jit(solution)/shard_map/ppermute | solution.py:41
  87.6 10.6 %collective-permute-start.31 = (bf16[64,1024]{1,0:T(8,128)(2,1)S(1)}, bf16[64,1024]{1,0:T(8,128)(2,1)S(1)}, u32[]{:S(2)}, u32[]{:S(2)}) collective-permute-start(bf16[64,1024]{1,0:T(8,128)(2,1)S(1)} %add_convert_fusion), channel_id=1, source_target_pairs={{0,24},{4,28},{8,16},{12,20},{16,8},{20,12},{24,0},{28,4},{1,25},{... | collective-permute-start | bytes 393224 | tf_op jit(solution)/shard_map/ppermute | solution.py:41
  (7 other events, 127.8 us)
